TPU v7x, 32 devices: a whole 2x2x4 slice. The times are simulated.
32 devices in a mesh: sp: 8 (over z, x), tp: 4 (over y, core).
Axes of the slice: x: 2, y: 2, z: 4, core: 2. Of those that a mesh axis runs over, the one named last changes fastest.
Arguments:
- conv_out: bfloat16 [1536, 2048], P('sp', 'tp'), may hold values from -6 to 6
- gate_in: bfloat16 [1536, 2048], P('sp', 'tp'), may hold values from -6 to 6
- block_states: float32 [8, 2048], P('sp', 'tp'), may hold values from -4 to 4
- decay_param: float32 [2048], P('tp'), may hold values from 4 to 20
- decay_shift: float32 [1536], P('sp'), may hold values from -2 to 0, as said below
- w_reset: bfloat16 [16, 128, 128], P('tp'), may hold values from -0.5 to 0.5
- w_input: bfloat16 [16, 128, 128], P('tp'), may hold values from -0.5 to 0.5
- w_out: bfloat16 [2048, 2048], P('tp'), may hold values from -0.125 to 0.125
- mixed: bfloat16 [1536, 2048], P('sp', 'tp'), may hold values from -6 to 6
- d_out: bfloat16 [1536, 2048], P('sp', 'tp'), may hold values from -6 to 6
- expert_ids: int32 [1536, 2], P('sp'), may hold values from 0 to 7, all different within a row; in each aligned block of 192 rows (0 to 191, 192 to 383, ...) at most 96 rows name the same one
- route_weights: float32 [1536, 2], P('sp'), may hold values from 0.2 to 1.4
- w_gate: bfloat16 [8, 2048, 1024], P('sp', None, 'tp'), may hold values from -0.125 to 0.125
- w_up: bfloat16 [8, 2048, 1024], P('sp', None, 'tp'), may hold values from -0.125 to 0.125
- w_down: bfloat16 [8, 1024, 2048], P('sp', 'tp'), may hold values from -0.1875 to 0.1875
Outputs:
- grad_w_gate: float32 [8, 2048, 1024], P('sp', None, 'tp')
- grad_w_up: float32 [8, 2048, 1024], P('sp', None, 'tp')
- grad_w_down: float32 [8, 1024, 2048], P('sp', 'tp')
- grad_out_proj_t: float32 [2048, 2048], P('sp', 'tp')
- recurrence_input_gradient: bfloat16 [1536, 2048], P('sp', 'tp')
- grad_gate: bfloat16 [1536, 2048], P('sp', 'tp')
Inputs may be any that keep to these rules, and one draw needn't show every extreme that they name: `expert_ids`: each row names 2 different experts; among the 192 tokens of one index of sp no expert is named more than 96 times, and in some index of sp one expert is named exactly 96 times. decay_shift is at most -0.05 / 1536 at every position.
All inputs are finite; a program needn't handle non-finite values.
Results may differ from a plain program's by a relative error of at most 0.013.
Values may be sent and summed in bfloat16 or wider, within the bound.
A program may use at most 128 MiB of HBM per device.

v0:
```python
import functools
import jax
import jax.numpy as jnp
from jax import lax
from jax.experimental import pallas as pl
from jax.experimental.pallas import tpu as pltpu
from jax.sharding import PartitionSpec as P

MESH = pl.DeviceIdType.MESH
GELU_C = 0.7978845608028654
GELU_K = 0.044715


def gelu_both(x):
    inner = jnp.tanh(GELU_C * (x + GELU_K * x * x * x))
    act = 0.5 * x * (1.0 + inner)
    slope = 0.5 * (1.0 + inner) + 0.5 * x * (1.0 - inner * inner) * (
        GELU_C * (1.0 + 3.0 * GELU_K * x * x)
    )
    return act, slope


def forward_kernel(
    conv_ref, gate_ref, bs_ref, slow_ref, shift_ref, wr_ref, wi_ref,
    merged_ref, reset_ref, inp_ref, dec_ref, norm_ref, st_ref, prev_ref, drive,
):
    rows = conv_ref.shape[0]
    width = wr_ref.shape[1]
    for h in range(wr_ref.shape[0]):
        cols = slice(h * width, (h + 1) * width)
        conv = conv_ref[:, cols]
        reset = jax.nn.sigmoid(jnp.dot(conv, wr_ref[h], preferred_element_type=jnp.float32))
        inp = jax.nn.sigmoid(jnp.dot(conv, wi_ref[h], preferred_element_type=jnp.float32))
        log_decay = -8.0 * reset * slow_ref[:, cols] + shift_ref[...]
        decays = jnp.exp(log_decay)
        norm = jnp.sqrt(-jnp.tanh(log_decay) * (decays * decays + 1.0))
        reset_ref[:, cols] = reset
        inp_ref[:, cols] = inp
        dec_ref[:, cols] = decays
        norm_ref[:, cols] = norm
        drive[:, cols] = norm * inp * conv.astype(jnp.float32)
    total = conv_ref.shape[1]
    row = lax.broadcasted_iota(jnp.int32, (8, total), 0)
    carry = bs_ref[...]
    for i in range(rows // 8):
        at = slice(8 * i, 8 * i + 8)
        a = dec_ref[at, :]
        b = drive[at, :]
        for d in (1, 2, 4):
            b = b + a * jnp.where(row >= d, pltpu.roll(b, d, 0), 0.0)
            a = a * jnp.where(row >= d, pltpu.roll(a, d, 0), 1.0)
        state = a * carry + b
        st_ref[at, :] = state
        prev_ref[at, :] = jnp.where(row >= 1, pltpu.roll(state, 1, 0), carry)
        carry = state[7:8, :]
    for h in range(wr_ref.shape[0]):
        cols = slice(h * width, (h + 1) * width)
        x = gate_ref[:, cols].astype(jnp.float32)
        inner = jnp.tanh(GELU_C * (x + GELU_K * x * x * x))
        merged_ref[:, cols] = (0.5 * x * (1.0 + inner) * st_ref[:, cols]).astype(jnp.bfloat16)


def backward_kernel(
    n, dm_ref, wo_ref, conv_ref, gate_ref, slow_ref, reset_ref, inp_ref, dec_ref, norm_ref,
    st_ref, prev_ref, wr_ref, wi_ref, blocks_ref,
    out_ref, gg_ref, got_ref,
    grad, prods, dstate, mine_pair, pairs, send_sem, recv_sem, block_send, block_recv,
):
    me = lax.axis_index("sp")
    barrier = pltpu.get_barrier_semaphore()
    for off in range(1, n):
        pl.semaphore_signal(
            barrier, inc=1, device_id={"sp": lax.rem(me + off, n)}, device_id_type=MESH
        )
    rows = conv_ref.shape[0]
    width = wr_ref.shape[1]
    total = conv_ref.shape[1]
    heads = wr_ref.shape[0]
    dstate[...] = lax.dot_general(
        dm_ref[...], wo_ref[...], (((1,), (1,)), ((), ())), preferred_element_type=jnp.float32
    )
    pl.semaphore_wait(barrier, n - 1)

    def block_to(peer, source):
        return pltpu.make_async_remote_copy(
            src_ref=blocks_ref.at[peer],
            dst_ref=got_ref.at[source],
            send_sem=block_send.at[0],
            recv_sem=block_recv.at[source],
            device_id={"sp": peer},
            device_id_type=MESH,
        )

    keep = pltpu.make_async_copy(blocks_ref.at[me], got_ref.at[me], block_send.at[1])
    keep.start()
    for off in range(1, n):
        block_to(lax.rem(me + off, n), me).start()
    for h in range(heads):
        cols = slice(h * width, (h + 1) * width)
        act, slope = gelu_both(gate_ref[:, cols].astype(jnp.float32))
        d_merged = dstate[:, cols]
        gg_ref[:, cols] = (d_merged * st_ref[:, cols] * slope).astype(jnp.bfloat16)
        dstate[:, cols] = d_merged * act
    row = lax.broadcasted_iota(jnp.int32, (8, total), 0)
    carry_g = jnp.zeros((1, total), jnp.float32)
    carry_p = jnp.ones((1, total), jnp.float32)
    following = jnp.ones((1, total), jnp.float32)
    for i in reversed(range(rows // 8)):
        at = slice(8 * i, 8 * i + 8)
        decay = dec_ref[at, :]
        a = jnp.where(row < 7, pltpu.roll(decay, 7, 0), following)
        following = decay[0:1, :]
        b = dstate[at, :]
        for d in (1, 2, 4):
            b = b + a * jnp.where(row < 8 - d, pltpu.roll(b, 8 - d, 0), 0.0)
            a = a * jnp.where(row < 8 - d, pltpu.roll(a, 8 - d, 0), 1.0)
        g = a * carry_g + b
        p = a * carry_p
        grad[at, :] = g
        prods[at, :] = p
        carry_g = g[0:1, :]
        carry_p = p[0:1, :]
    mine_pair[0:1, :] = carry_p * following
    mine_pair[1:2, :] = carry_g * following
    mine_pair[2:8, :] = jnp.zeros((6, total), jnp.float32)
    pairs[me] = jnp.zeros((8, total), jnp.float32)

    def copy_to(peer, source):
        return pltpu.make_async_remote_copy(
            src_ref=mine_pair,
            dst_ref=pairs.at[source],
            send_sem=send_sem.at[0],
            recv_sem=recv_sem.at[source],
            device_id={"sp": peer},
            device_id_type=MESH,
        )

    for off in range(1, n):
        copy_to(lax.rem(me + off, n), me).start()
    for off in range(1, n):
        copy_to(lax.rem(me + off, n), lax.rem(me + off, n)).wait_recv()
    for off in range(1, n):
        copy_to(lax.rem(me + off, n), me).wait_send()
    enter = jnp.zeros((1, total), jnp.float32)
    for p in reversed(range(n)):
        pair = pairs[p]
        enter = jnp.where(p > me, pair[1:2, :] + pair[0:1, :] * enter, enter)
    for h in range(heads):
        cols = slice(h * width, (h + 1) * width)
        state_grad = grad[:, cols] + prods[:, cols] * enter[:, cols]
        conv = conv_ref[:, cols].astype(jnp.float32)
        inp, norm = inp_ref[:, cols], norm_ref[:, cols]
        decays, reset = dec_ref[:, cols], reset_ref[:, cols]
        d_log = state_grad * decays * prev_ref[:, cols] - (
            state_grad * inp * conv * decays * decays / norm
        )
        d_r = (d_log * (-8.0 * slow_ref[:, cols]) * reset * (1.0 - reset)).astype(jnp.bfloat16)
        d_i = (state_grad * norm * conv * inp * (1.0 - inp)).astype(jnp.bfloat16)
        out_ref[:, cols] = (
            state_grad * norm * inp
            + lax.dot_general(d_r, wr_ref[h], (((1,), (1,)), ((), ())), preferred_element_type=jnp.float32)
            + lax.dot_general(d_i, wi_ref[h], (((1,), (1,)), ((), ())), preferred_element_type=jnp.float32)
        ).astype(jnp.bfloat16)
    keep.wait()
    for off in range(1, n):
        peer = lax.rem(me + off, n)
        block_to(peer, peer).wait_recv()
        block_to(peer, me).wait_send()


VM = pl.BlockSpec(memory_space=pltpu.VMEM)


def run_forward(conv_out, gate_in, block_states, slow, shift, w_reset, w_input):
    shape = conv_out.shape
    full = jax.ShapeDtypeStruct(shape, jnp.float32)
    return pl.pallas_call(
        forward_kernel,
        out_shape=(jax.ShapeDtypeStruct(shape, jnp.bfloat16),) + (full,) * 6,
        in_specs=[VM] * 7,
        out_specs=(VM,) * 7,
        scratch_shapes=[pltpu.VMEM(shape, jnp.float32)],
        cost_estimate=pl.CostEstimate(flops=200_000_000, bytes_accessed=16_000_000, transcendentals=0),
    )(conv_out, gate_in, block_states, slow, shift, w_reset, w_input)


def run_backward(n, *args):
    shape = args[2].shape
    half = jax.ShapeDtypeStruct(shape, jnp.bfloat16)
    return pl.pallas_call(
        functools.partial(backward_kernel, n),
        out_shape=(half, half, jax.ShapeDtypeStruct(args[-1].shape, jnp.bfloat16)),
        in_specs=[VM] * len(args),
        out_specs=(VM, VM, pl.BlockSpec(memory_space=pl.ANY)),
        scratch_shapes=[pltpu.VMEM(shape, jnp.float32)] * 3
        + [
            pltpu.VMEM((8, shape[1]), jnp.float32),
            pltpu.VMEM((n, 8, shape[1]), jnp.float32),
            pltpu.SemaphoreType.DMA((1,)),
            pltpu.SemaphoreType.DMA((n,)),
            pltpu.SemaphoreType.DMA((2,)),
            pltpu.SemaphoreType.DMA((n,)),
        ],
        compiler_params=pltpu.CompilerParams(collective_id=0, has_side_effects=True),
        cost_estimate=pl.CostEstimate(flops=400_000_000, bytes_accessed=40_000_000, transcendentals=0),
    )(*args)


def dispatch_kernel(
    n, width, mixed_ref, cot_ref, ids_ref, wts_ref, merged_ref,
    rows_out, cots_out, merged_out,
    send_rows, send_cots, send_sem, local_sem, sp_sem, y_sem, own_sem, fwd_sem, merged_sem,
):
    me, q = lax.axis_index("sp"), lax.axis_index("tp")
    near, far = q ^ 1, q ^ 2
    barrier = pltpu.get_barrier_semaphore()
    for off in range(1, n):
        pl.semaphore_signal(
            barrier, inc=1, device_id={"sp": lax.rem(me + off, n)}, device_id_type=MESH
        )
    for other in (near, far):
        pl.semaphore_signal(barrier, inc=1, device_id={"tp": other}, device_id_type=MESH)
    tokens = mixed_ref.shape[0]
    slots = send_rows.shape[1]
    top = ids_ref.shape[0]
    named = lax.broadcasted_iota(jnp.int32, (n, tokens), 0)
    member = jnp.zeros((n, tokens), jnp.float32)
    weight = jnp.zeros((n, tokens), jnp.float32)
    for k in range(top):
        hit = ids_ref[k : k + 1, :] == named
        member = jnp.where(hit, 1.0, member)
        weight = jnp.where(hit, wts_ref[k : k + 1, :], weight)
    earlier = lax.broadcasted_iota(jnp.int32, (tokens, tokens), 0) < (
        lax.broadcasted_iota(jnp.int32, (tokens, tokens), 1)
    )
    rank = jnp.dot(
        member.astype(jnp.bfloat16),
        jnp.where(earlier, 1.0, 0.0).astype(jnp.bfloat16),
        preferred_element_type=jnp.float32,
    )
    rank = jnp.where(member > 0.5, rank, -1.0).astype(jnp.int32)
    place = lax.broadcasted_iota(jnp.int32, (slots, tokens), 0)
    pl.semaphore_wait(barrier, n + 1)
    sent = []

    def start(copy):
        copy.start()
        sent.append(copy)

    def cols(of):
        return pl.ds(pl.multiple_of(of * width, width), width)

    def remote(src, dst, recv, where):
        return pltpu.make_async_remote_copy(
            src_ref=src, dst_ref=dst, send_sem=send_sem.at[0], recv_sem=recv,
            device_id=where, device_id_type=MESH,
        )

    def merged_copy(peer, source):
        return remote(merged_ref, merged_out.at[source], merged_sem.at[source], {"sp": peer})

    for e in range(n):
        chosen = place == rank[e : e + 1, :]
        pick = jnp.where(chosen, 1.0, 0.0)
        scale = jnp.sum(jnp.where(chosen, weight[e : e + 1, :], 0.0), axis=1, keepdims=True)
        pick = pick.astype(jnp.bfloat16)
        send_rows[e] = jnp.dot(
            pick, mixed_ref[...], preferred_element_type=jnp.float32
        ).astype(jnp.bfloat16)
        send_cots[e] = (
            scale * jnp.dot(pick, cot_ref[...], preferred_element_type=jnp.float32)
        ).astype(jnp.bfloat16)
    pieces = ((send_rows, rows_out, 0), (send_cots, cots_out, 1))

    def over_sp(peer, source, piece):
        buffer, out, i = piece
        return remote(
            buffer.at[peer], out.at[source, :, cols(q)], sp_sem.at[i, source], {"sp": peer}
        )

    def over_tp(source, owner, other, sems, piece):
        _, out, i = piece
        spot = out.at[source, :, cols(owner)]
        return remote(spot, spot, sems.at[i, source], {"tp": other})

    own = [
        pltpu.make_async_copy(b.at[me], out.at[me, :, cols(q)], local_sem.at[0])
        for b, out, _ in pieces
    ]
    for copy in own:
        copy.start()
    for off in range(1, n):
        peer = lax.rem(me + off, n)
        for piece in pieces:
            start(over_sp(peer, me, piece))
    for copy in own:
        copy.wait()
    keep = pltpu.make_async_copy(merged_ref, merged_out.at[me], local_sem.at[0])
    keep.start()
    for off in range(1, n):
        start(merged_copy(lax.rem(me + off, n), me))
    order = [lax.rem(me + n - off, n) for off in range(n)]

    def relay(source):
        for piece in pieces:
            over_tp(source, far, far, y_sem, piece).wait_recv()
            start(over_tp(source, far, near, fwd_sem, piece))

    for i, source in enumerate(order):
        for piece in pieces:
            if i > 0:
                over_sp(source, source, piece).wait_recv()
            start(over_tp(source, q, far, y_sem, piece))
            start(over_tp(source, q, near, own_sem, piece))
        if i > 0:
            relay(order[i - 1])
    relay(order[-1])
    keep.wait()
    for i, source in enumerate(order):
        for piece in pieces:
            over_tp(source, near, near, own_sem, piece).wait_recv()
            over_tp(source, near ^ 2, near, fwd_sem, piece).wait_recv()
        if i > 0:
            merged_copy(source, source).wait_recv()
    for copy in sent:
        copy.wait_send()


def run_dispatch(n, parts, slots, mixed, cot, ids, weights, merged):
    tokens, width = mixed.shape
    got = jax.ShapeDtypeStruct((n, slots, width * parts), jnp.bfloat16)
    anywhere = pl.BlockSpec(memory_space=pl.ANY)
    dma = pltpu.SemaphoreType.DMA
    return pl.pallas_call(
        functools.partial(dispatch_kernel, n, width),
        out_shape=(got, got, jax.ShapeDtypeStruct((n, tokens, width), jnp.bfloat16)),
        in_specs=[VM] * 5,
        out_specs=(anywhere,) * 3,
        scratch_shapes=[pltpu.VMEM((n, slots, width), jnp.bfloat16)] * 2
        + [dma((1,)), dma((1,)), dma((2, n)), dma((2, n)), dma((2, n)), dma((2, n)), dma((n,))],
        compiler_params=pltpu.CompilerParams(collective_id=1, has_side_effects=True),
        cost_estimate=pl.CostEstimate(flops=800_000_000, bytes_accessed=80_000_000, transcendentals=0),
    )(mixed, cot, ids, weights, merged)


def over_rows(left_matrix, right_matrix):
    return lax.dot_general(
        left_matrix, right_matrix, (((0,), (0,)), ((), ())), preferred_element_type=jnp.float32
    )


def against_rows(left_matrix, right_matrix):
    return lax.dot_general(
        left_matrix, right_matrix, (((1,), (1,)), ((), ())), preferred_element_type=jnp.float32
    )


def slot_places(expert_ids, experts, slots):
    tok_rows, top_k = expert_ids.shape
    flat_ids = expert_ids.reshape(-1)
    onehot = (flat_ids[:, None] == jnp.arange(experts, dtype=jnp.int32)[None, :]).astype(jnp.int32)
    slot_rank = jnp.sum((jnp.cumsum(onehot, axis=0) - 1) * onehot, axis=1)
    return flat_ids * slots + slot_rank


def expert_terms(expert_in, expert_cot, gate_matrix, up_matrix, down_matrix):
    up_pre = jnp.dot(expert_in, gate_matrix, preferred_element_type=jnp.float32)
    linear = jnp.dot(expert_in, up_matrix, preferred_element_type=jnp.float32)
    sigmoid_up = jax.nn.sigmoid(up_pre)
    silu_up = up_pre * sigmoid_up
    hidden_state = (silu_up * linear).astype(jnp.bfloat16)
    d_hidden = against_rows(expert_cot, down_matrix)
    d_linear = (d_hidden * silu_up).astype(jnp.bfloat16)
    d_up = (d_hidden * linear * sigmoid_up * (1.0 + up_pre * (1.0 - sigmoid_up))).astype(
        jnp.bfloat16
    )
    grad_gate_e = over_rows(expert_in, d_up)
    grad_up_e = over_rows(expert_in, d_linear)
    grad_down_e = over_rows(hidden_state, expert_cot)
    partial_value = against_rows(d_up, gate_matrix) + against_rows(d_linear, up_matrix)
    return (grad_gate_e, grad_up_e, grad_down_e, partial_value)


def body(
    conv_out,
    gate_in,
    block_states,
    decay_param,
    decay_shift,
    w_reset,
    w_input,
    w_out,
    mixed,
    d_out,
    expert_ids,
    route_weights,
    w_gate,
    w_up,
    w_down,
):
    tok_rows, top_k = expert_ids.shape
    experts = lax.axis_size("sp")
    capacity = 2 * tok_rows * top_k // experts
    slow_rate = jax.nn.softplus(-decay_param)[None, :]
    merged_in, reset, input_gate, decays, norm_in, states, prev_states = run_forward(
        conv_out, gate_in, block_states, slow_rate, decay_shift[:, None], w_reset, w_input
    )
    slots = -(-capacity // 16) * 16
    slot_index = slot_places(expert_ids, experts, slots)
    got_rows, got_cot, merged_full = run_dispatch(
        experts, lax.axis_size("tp"), slots, mixed, d_out, expert_ids.T, route_weights.T, merged_in
    )
    width_full = got_cot.shape[2]
    grad_gate_e, grad_up_e, grad_down_e, partial_value = expert_terms(
        got_rows.reshape(-1, width_full),
        got_cot.reshape(-1, width_full),
        w_gate[0],
        w_up[0],
        w_down[0],
    )
    row_grad = lax.psum_scatter(
        partial_value.astype(jnp.bfloat16), "tp", scatter_dimension=1, tiled=True
    )
    columns = row_grad.shape[1]
    returned = lax.all_to_all(
        row_grad.reshape(experts, slots, columns), "sp", split_axis=0, concat_axis=0, tiled=True
    )
    summed = jnp.sum(
        returned.reshape(-1, columns)[slot_index]
        .astype(jnp.float32)
        .reshape(tok_rows, top_k, columns),
        axis=1,
    )
    d_columns = (d_out.astype(jnp.float32) + summed).astype(jnp.bfloat16)
    d_mixed = lax.all_gather(d_columns, "tp", axis=1, tiled=True)
    blocks = d_mixed.reshape(tok_rows, experts, -1).transpose(1, 0, 2)
    recurrence_input_gradient, grad_gate, got_blocks = run_backward(
        experts, d_mixed, w_out, conv_out, gate_in, slow_rate, reset, input_gate, decays, norm_in,
        states, prev_states, w_reset, w_input, blocks,
    )
    grad_out_proj_t = over_rows(
        got_blocks.reshape(experts * tok_rows, -1), merged_full.reshape(experts * tok_rows, -1)
    )
    return (
        grad_gate_e[None],
        grad_up_e[None],
        grad_down_e[None],
        grad_out_proj_t,
        recurrence_input_gradient,
        grad_gate,
    )


def solution(mesh):
    placed = (
        P("sp", "tp"),
        P("sp", "tp"),
        P("sp", "tp"),
        P("tp"),
        P("sp"),
        P("tp", None, None),
        P("tp", None, None),
        P("tp", None),
        P("sp", "tp"),
        P("sp", "tp"),
        P("sp", None),
        P("sp", None),
        P("sp", None, "tp"),
        P("sp", None, "tp"),
        P("sp", "tp", None),
    )
    return jax.shard_map(
        body,
        mesh=mesh,
        in_specs=placed,
        out_specs=(
            P("sp", None, "tp"),
            P("sp", None, "tp"),
            P("sp", "tp", None),
            P("sp", "tp"),
            P("sp", "tp"),
            P("sp", "tp"),
        ),
        check_vma=False,
    )
```

profile of v0, /device:TPU:0, one launch (start us, length us, event | category | flops | bytes accessed | tf_op | source)
XLA Modules:
  0.0 217.3 jit_solution(3127269125950922207)
XLA Ops:
  7.2 1.4 compare_select_fusion.1
  8.6 1.4 copy.21.shift_ref
  10.0 3.5 %shard_map.190 = (bf16[192,512]{1,0:T(8,128)(2,1)}, f32[192,512]{1,0:T(8,128)}, f32[192,512]{1,0:T(8,128)}, f32[192,512]{1,0:T(8,128)}, f32[192,512]{1,0:T(8,128...) custom-call(bf16[192,512]{1,0:T(8,128)(2,1)} %conv_ref.3, bf16[192,512]{1,0:T(8,128)(2,1)} %gate_ref.3, f32[1,512]{1,0:T(1,128)} %bs_ref.1, ...), custom_call_target="tpu_custom_call" | custom-call | flops 200000000 | bytes 16000000 | tf_op jit(solution)/shard_map/pallas_call | solution.py:177
  13.5 65.5 %shard_map.191 = (bf16[8,96,2048]{2,1,0:T(8,128)(2,1)}, bf16[8,96,2048]{2,1,0:T(8,128)(2,1)}, bf16[8,192,512]{2,1,0:T(8,128)(2,1)}) custom-call(bf16[192,512]{1,0:T(8,128)(2,1)} %mixed_ref.1, bf16[192,512]{1,0:T(8,128)(2,1)} %cot_ref.1, s32[2,192]{1,0:T(2,128)} %bitcast.63, f32[2,192]{1,0:T(2,128)} %bitcast.66, bf16[192,512]{1,0:T(8,128)(2,1)} %get-tuple-element.19.merged_ref), custom_call_target="tpu_custom_call" | custom-call | flops 800000000 | bytes 80000000 | tf_op jit(solution)/shard_map/pallas_call | solution.py:334
  79.0 3.0 %fusion.2 = f32[768,256]{1,0:T(8,128)S(1)} fusion(bf16[768,2048]{1,0:T(8,128)(2,1)} %bitcast.69, bf16[1,2048,256]{2,1,0:T(8,128)(2,1)S(1)} %copy-done), kind=kOutput, calls=%fused_computation.8 | convolution fusion | flops 805306368 | bytes 4980736 | tf_op jit(solution)/shard_map/dot_general | solution.py:367
  82.1 1.0 fusion.5
  83.2 0.2 copy-done.7
  83.4 1.3 copy-done.8
  84.6 1.2 multiply_convert_fusion.1
  85.9 1.0 fusion
  86.9 2.8 %add_convert_fusion = bf16[768,2048]{1,0:T(8,128)(2,1)} fusion(f32[768,2048]{1,0:T(8,128)S(1)} %fusion, bf16[768,256]{1,0:T(8,128)(2,1)S(1)} %get-tuple-element.32, bf16[1,2048,256]{2,1,0:T(8,128)(2,1)S(1)} %copy-done.3), kind=kOutput, calls=%fused_computation.1 | convolution fusion | flops 808452096 | bytes 10878976 | tf_op jit(solution)/shard_map/dot_general | solution.py:353
  89.7 0.7 copy-done.6
  90.5 0.1 eq.29
  90.9 0.1 mul.49
  91.0 0.9 reduce-window.6
  91.9 0.2 slice_reduce_fusion
  92.3 46.8 %reduce-scatter.2.cloned.1.call-done = bf16[768,512]{1,0:T(8,128)(2,1)} async-done(((bf16[768,2048]{1,0:T(8,128)(2,1)}), bf16[768,512]{1,0:T(8,128)(2,1)}) %reduce-scatter.2.cloned.1.call-update) | async-done | bytes 786448 | tf_op jit(solution)/shard_map/reduce_scatter | solution.py:421
  139.0 5.5 %all-to-all-start = ((bf16[8,96,512]{2,1,0:T(8,128)(2,1)}), bf16[8,96,512]{2,1,0:T(8,128)(2,1)S(1)}, u32[]{:S(2)}, u32[]{:S(2)}) async-start(bf16[8,96,512]{2,1,0:T(8,128)(2,1)} %bitcast.60), calls=%async_computation.1 | async-start | bytes 1572864 | tf_op jit(solution)/shard_map/all_to_all | solution.py:425
  144.6 4.4 %convolution_bitcast_fusion.2 = f32[1,2048,256]{2,1,0:T(8,128)} fusion(bf16[768,2048]{1,0:T(8,128)(2,1)} %bitcast.70, bf16[768,256]{1,0:T(8,128)(2,1)S(1)} %get-tuple-element.33), kind=kOutput, calls=%fused_computation.4 | convolution fusion | flops 805306368 | bytes 5636096 | tf_op jit(solution)/shard_map/dot_general | solution.py:347
  149.0 2.4 %convolution_bitcast_fusion.1 = f32[1,2048,256]{2,1,0:T(8,128)} fusion(bf16[768,2048]{1,0:T(8,128)(2,1)S(1)} %bitcast.72, bf16[768,256]{1,0:T(8,128)(2,1)S(1)} %get-tuple-element.32), kind=kOutput, calls=%fused_computation.3 | convolution fusion | flops 805306368 | bytes 5636096 | tf_op jit(solution)/shard_map/dot_general | solution.py:347
  151.4 2.4 %convolution_bitcast_fusion = f32[1,256,2048]{2,1,0:T(8,128)} fusion(bf16[768,2048]{1,0:T(8,128)(2,1)S(1)} %bitcast.68, f32[768,256]{1,0:T(8,128)S(1)} %copy-done.13, f32[768,256]{1,0:T(8,128)S(1)} %fusion.2), kind=kOutput, calls=%fused_computation.2 | convolution fusion | flops 806486016 | bytes 6815744 | tf_op jit(solution)/shard_map/dot_general | solution.py:347
  153.8 10.8 %all-to-all-done = bf16[8,96,512]{2,1,0:T(8,128)(2,1)S(1)} async-done(((bf16[8,96,512]{2,1,0:T(8,128)(2,1)}), bf16[8,96,512]{2,1,0:T(8,128)(2,1)S(1)}, u32[]{:S(2)}, u32[]{:S(2)}) %all-to-all-start) | async-done | bytes 786464 | tf_op jit(solution)/shard_map/all_to_all | solution.py:425
  164.6 2.1 gather_fusion
  166.7 0.5 reshape.87
  167.2 0.9 reduce_sum.22
  168.2 7.7 %all_gather.3.dm_ref = bf16[192,2048]{1,0:T(8,128)(2,1)S(1)} all-gather(bf16[192,512]{1,0:T(8,128)(2,1)S(1)} %add_convert_fusion.1), channel_id=1, replica_groups=mesh['sp'=8,'tp'=4] {'tp'}, dimensions={1}, use_global_device_ids=true | all-gather | bytes 983040 | tf_op jit(solution)/shard_map/all_gather | solution.py:435
  175.8 1.0 copy.28
  176.8 0.2 copy-done.1
  177.0 28.5 %shard_map.192 = (bf16[192,512]{1,0:T(8,128)(2,1)}, bf16[192,512]{1,0:T(8,128)(2,1)}, bf16[8,192,256]{2,1,0:T(8,128)(2,1)}) custom-call(bf16[192,2048]{1,0:T(8,128)(2,1)} %copy-done.1, bf16[512,2048]{1,0:T(8,128)(2,1)} %wo_ref.1, bf16[192,512]{1,0:T(8,128)(2,1)} %conv_ref.3, bf16[192,512]{1,0:T(8,128)(2,1)} %gate_ref.3, f32[1,512]{1,0:T(1,128)} %bitcast.62, ...), custom_call_target="tpu_custom_call" | custom-call | flops 400000000 | bytes 40000000 | tf_op jit(solution)/shard_map/pallas_call | solution.py:190
  205.6 2.6 %convolution_bitcast_fusion.3 = f32[256,512]{1,0:T(8,128)} fusion(bf16[8,192,256]{2,1,0:T(8,128)(2,1)} %get-tuple-element.28, bf16[8,192,512]{2,1,0:T(8,128)(2,1)S(1)} %copy-done.2), kind=kOutput, calls=%fused_computation.5 | convolution fusion | flops 402653184 | bytes 2883584 | tf_op jit(solution)/shard_map/dot_general | solution.py:347
  208.1 1.6 copy.31
  209.7 0.7 copy.32
  (36 shorter events, 0.8 us)
Async XLA Ops:
  7.2 71.8 %copy-start = (bf16[1,2048,256]{2,1,0:T(8,128)(2,1)S(1)}, bf16[1,2048,256]{2,1,0:T(8,128)(2,1)}, u32[]{:S(2)}) copy-start(bf16[1,2048,256]{2,1,0:T(8,128)(2,1)} %param.27) | copy-start | bytes 3145732
  7.2 131.9 %reduce-scatter.2.cloned.1.call-start = ((), (), s32[]{:S(2)}) async-start(), calls=%async_computation.2 | async-start | bytes 3932160 | tf_op jit(solution)/shard_map/reduce_scatter | solution.py:421
  79.0 3.1 %copy-start.3 = (bf16[1,2048,256]{2,1,0:T(8,128)(2,1)S(1)}, bf16[1,2048,256]{2,1,0:T(8,128)(2,1)}, u32[]{:S(2)}) copy-start(bf16[1,2048,256]{2,1,0:T(8,128)(2,1)} %param.28) | copy-start | bytes 3145732
  79.0 3.2 %copy-start.10 = (bf16[8,96,2048]{2,1,0:T(8,128)(2,1)S(1)}, bf16[8,96,2048]{2,1,0:T(8,128)(2,1)}, u32[]{:S(2)}) copy-start(bf16[8,96,2048]{2,1,0:T(8,128)(2,1)} %get-tuple-element.20) | copy-start | bytes 9437188
  82.1 1.2 copy-start.7
  82.1 2.5 %copy-start.8 = (bf16[8,96,2048]{2,1,0:T(8,128)(2,1)S(1)}, bf16[8,96,2048]{2,1,0:T(8,128)(2,1)}, u32[]{:S(2)}) copy-start(bf16[8,96,2048]{2,1,0:T(8,128)(2,1)} %get-tuple-element.21) | copy-start | bytes 9437188
  83.1 2.7 %copy-start.12 = (f32[768,256]{1,0:T(8,128)}, f32[768,256]{1,0:T(8,128)S(1)}, u32[]{:S(2)}) copy-start(f32[768,256]{1,0:T(8,128)S(1)} %fusion.5) | copy-start | bytes 2359300
  89.7 0.7 copy-start.6
  139.0 25.6 %all-to-all-start = ((bf16[8,96,512]{2,1,0:T(8,128)(2,1)}), bf16[8,96,512]{2,1,0:T(8,128)(2,1)S(1)}, u32[]{:S(2)}, u32[]{:S(2)}) async-start(bf16[8,96,512]{2,1,0:T(8,128)(2,1)} %bitcast.60), calls=%async_computation.1 | async-start | bytes 1572864 | tf_op jit(solution)/shard_map/all_to_all | solution.py:425
  144.6 4.4 %copy-start.11 = (bf16[8,96,2048]{2,1,0:T(8,128)(2,1)S(1)}, bf16[8,96,2048]{2,1,0:T(8,128)(2,1)}, u32[]{:S(2)}) copy-start(bf16[8,96,2048]{2,1,0:T(8,128)(2,1)} %get-tuple-element.20) | copy-start | bytes 9437188
  149.0 2.4 %copy-start.9 = (bf16[8,96,2048]{2,1,0:T(8,128)(2,1)S(1)}, bf16[8,96,2048]{2,1,0:T(8,128)(2,1)}, u32[]{:S(2)}) copy-start(bf16[8,96,2048]{2,1,0:T(8,128)(2,1)} %get-tuple-element.21) | copy-start | bytes 9437188
  149.0 2.4 %copy-start.13 = (f32[768,256]{1,0:T(8,128)S(1)}, f32[768,256]{1,0:T(8,128)}, u32[]{:S(2)}) copy-start(f32[768,256]{1,0:T(8,128)} %copy-done.12) | copy-start | bytes 2359300
  153.8 14.4 %copy-start.5 = (bf16[192,512]{1,0:T(8,128)(2,1)S(1)}, bf16[192,512]{1,0:T(8,128)(2,1)}, u32[]{:S(2)}) copy-start(bf16[192,512]{1,0:T(8,128)(2,1)} %cot_ref.1) | copy-start | bytes 589828
  175.8 1.2 copy-start.1
  177.0 28.5 %copy-start.2 = (bf16[8,192,512]{2,1,0:T(8,128)(2,1)S(1)}, bf16[8,192,512]{2,1,0:T(8,128)(2,1)}, u32[]{:S(2)}) copy-start(bf16[8,192,512]{2,1,0:T(8,128)(2,1)} %get-tuple-element.29) | copy-start | bytes 4718596
  205.6 4.2 %copy-start.4 = (bf16[192,512]{1,0:T(8,128)(2,1)S(1)}, bf16[192,512]{1,0:T(8,128)(2,1)}, u32[]{:S(2)}) copy-start(bf16[192,512]{1,0:T(8,128)(2,1)} %get-tuple-element.45) | copy-start | bytes 589828
Sparse Core Ops, SparseCore 0:
  89.8 49.1 reduce-scatter.1
where the time goes:
time: 218 us; the launch traced here: 217 us
  Pallas kernels  97.5 us (45%)
  waiting for transfers between devices  57.6 us (26%)
  matrix products  20.7 us (9%)
  between operations  14.2 us (7%)
  local copies, waits for them, and re-layouts  10.6 us (5%)
  blocking collectives  7.66 us (4%)
  starting transfers between devices  5.54 us (3%)
  other arithmetic  3.36 us (2%)
    pallas_call x1, Pallas kernels, run_dispatch(): pl.pallas_call(functools.partial(dispatch_kernel, n, width), out_shape=(g...  65.5 us
    reduce_scatter x1, waiting for transfers between devices, body(): lax.psum_scatter(partial_value.astype(jnp.bfloat16), 'tp', scatter_dimens...  46.8 us
    pallas_call x1, Pallas kernels, run_backward(): pl.pallas_call(functools.partial(backward_kernel, n), out_shape=(half, ha...  28.5 us
    dot_general x4, matrix products, over_rows(): lax.dot_general(left_matrix, right_matrix, (((0,), (0,)), ((), ())), pref...  11.7 us
    all_to_all x1, waiting for transfers between devices, body(): lax.all_to_all(row_grad.reshape(experts, slots, columns), 'sp', split_axi...  10.8 us
    all_gather x1, blocking collectives, body(): d_mixed = lax.all_gather(d_columns, 'tp', axis=1, tiled=True)  7.66 us
    all_to_all x1, starting transfers between devices, body(): lax.all_to_all(row_grad.reshape(experts, slots, columns), 'sp', split_axi...  5.51 us
    dot_general x3, matrix products, against_rows(): lax.dot_general(left_matrix, right_matrix, (((1,), (1,)), ((), ())), pref...  4.99 us
  transfers between devices with their start and end apart: 2, of which 2 were waited for; matrix products, arithmetic and copies ran while one was open for 5% of the time, Pallas kernels for 0%

commit v1 on v0

v1 whole, which is shorter than its diff:
```python
import functools
import jax
import jax.numpy as jnp
from jax import lax
from jax.experimental import pallas as pl
from jax.experimental.pallas import tpu as pltpu
from jax.sharding import PartitionSpec as P

MESH = pl.DeviceIdType.MESH
GELU_C = 0.7978845608028654
GELU_K = 0.044715


def gelu_both(x):
    inner = jnp.tanh(GELU_C * (x + GELU_K * x * x * x))
    act = 0.5 * x * (1.0 + inner)
    slope = 0.5 * (1.0 + inner) + 0.5 * x * (1.0 - inner * inner) * (
        GELU_C * (1.0 + 3.0 * GELU_K * x * x)
    )
    return act, slope


def recurrence_forward(
    conv_ref, gate_ref, bs_ref, slow, shift, wr_ref, wi_ref,
    merged_ref, reset_ref, inp_ref, dec_ref, norm_ref, st_ref, prev_ref, drive,
):
    rows = conv_ref.shape[0]
    width = wr_ref.shape[1]
    for h in range(wr_ref.shape[0]):
        cols = slice(h * width, (h + 1) * width)
        conv = conv_ref[:, cols]
        reset = jax.nn.sigmoid(jnp.dot(conv, wr_ref[h], preferred_element_type=jnp.float32))
        inp = jax.nn.sigmoid(jnp.dot(conv, wi_ref[h], preferred_element_type=jnp.float32))
        log_decay = -8.0 * reset * slow[:, cols] + shift
        decays = jnp.exp(log_decay)
        norm = jnp.sqrt(-jnp.tanh(log_decay) * (decays * decays + 1.0))
        reset_ref[:, cols] = reset
        inp_ref[:, cols] = inp
        dec_ref[:, cols] = decays
        norm_ref[:, cols] = norm
        drive[:, cols] = norm * inp * conv.astype(jnp.float32)
    total = conv_ref.shape[1]
    row = lax.broadcasted_iota(jnp.int32, (8, total), 0)
    carry = bs_ref[...]
    for i in range(rows // 8):
        at = slice(8 * i, 8 * i + 8)
        a = dec_ref[at, :]
        b = drive[at, :]
        for d in (1, 2, 4):
            b = b + a * jnp.where(row >= d, pltpu.roll(b, d, 0), 0.0)
            a = a * jnp.where(row >= d, pltpu.roll(a, d, 0), 1.0)
        state = a * carry + b
        st_ref[at, :] = state
        prev_ref[at, :] = jnp.where(row >= 1, pltpu.roll(state, 1, 0), carry)
        carry = state[7:8, :]
    for h in range(wr_ref.shape[0]):
        cols = slice(h * width, (h + 1) * width)
        x = gate_ref[:, cols].astype(jnp.float32)
        inner = jnp.tanh(GELU_C * (x + GELU_K * x * x * x))
        merged_ref[:, cols] = (0.5 * x * (1.0 + inner) * st_ref[:, cols]).astype(jnp.bfloat16)


def backward_kernel(
    n, dm_ref, wo_ref, conv_ref, gate_ref, slow_ref, reset_ref, inp_ref, dec_ref, norm_ref,
    st_ref, prev_ref, wr_ref, wi_ref, blocks_ref,
    out_ref, gg_ref, got_ref,
    grad, prods, dstate, mine_pair, pairs, send_sem, recv_sem, block_send, block_recv,
):
    me = lax.axis_index("sp")
    barrier = pltpu.get_barrier_semaphore()
    for off in range(1, n):
        pl.semaphore_signal(
            barrier, inc=1, device_id={"sp": lax.rem(me + off, n)}, device_id_type=MESH
        )
    rows = conv_ref.shape[0]
    width = wr_ref.shape[1]
    total = conv_ref.shape[1]
    heads = wr_ref.shape[0]
    dstate[...] = lax.dot_general(
        dm_ref[...], wo_ref[...], (((1,), (1,)), ((), ())), preferred_element_type=jnp.float32
    )
    pl.semaphore_wait(barrier, n - 1)

    def block_to(peer, source):
        return pltpu.make_async_remote_copy(
            src_ref=blocks_ref.at[peer],
            dst_ref=got_ref.at[source],
            send_sem=block_send.at[0],
            recv_sem=block_recv.at[source],
            device_id={"sp": peer},
            device_id_type=MESH,
        )

    keep = pltpu.make_async_copy(blocks_ref.at[me], got_ref.at[me], block_send.at[1])
    keep.start()
    for off in range(1, n):
        block_to(lax.rem(me + off, n), me).start()
    for h in range(heads):
        cols = slice(h * width, (h + 1) * width)
        act, slope = gelu_both(gate_ref[:, cols].astype(jnp.float32))
        d_merged = dstate[:, cols]
        gg_ref[:, cols] = (d_merged * st_ref[:, cols] * slope).astype(jnp.bfloat16)
        dstate[:, cols] = d_merged * act
    row = lax.broadcasted_iota(jnp.int32, (8, total), 0)
    carry_g = jnp.zeros((1, total), jnp.float32)
    carry_p = jnp.ones((1, total), jnp.float32)
    following = jnp.ones((1, total), jnp.float32)
    for i in reversed(range(rows // 8)):
        at = slice(8 * i, 8 * i + 8)
        decay = dec_ref[at, :]
        a = jnp.where(row < 7, pltpu.roll(decay, 7, 0), following)
        following = decay[0:1, :]
        b = dstate[at, :]
        for d in (1, 2, 4):
            b = b + a * jnp.where(row < 8 - d, pltpu.roll(b, 8 - d, 0), 0.0)
            a = a * jnp.where(row < 8 - d, pltpu.roll(a, 8 - d, 0), 1.0)
        g = a * carry_g + b
        p = a * carry_p
        grad[at, :] = g
        prods[at, :] = p
        carry_g = g[0:1, :]
        carry_p = p[0:1, :]
    mine_pair[0:1, :] = carry_p * following
    mine_pair[1:2, :] = carry_g * following
    mine_pair[2:8, :] = jnp.zeros((6, total), jnp.float32)
    pairs[me] = jnp.zeros((8, total), jnp.float32)

    def copy_to(peer, source):
        return pltpu.make_async_remote_copy(
            src_ref=mine_pair,
            dst_ref=pairs.at[source],
            send_sem=send_sem.at[0],
            recv_sem=recv_sem.at[source],
            device_id={"sp": peer},
            device_id_type=MESH,
        )

    for off in range(1, n):
        copy_to(lax.rem(me + off, n), me).start()
    for off in range(1, n):
        copy_to(lax.rem(me + off, n), lax.rem(me + off, n)).wait_recv()
    for off in range(1, n):
        copy_to(lax.rem(me + off, n), me).wait_send()
    enter = jnp.zeros((1, total), jnp.float32)
    for p in reversed(range(n)):
        pair = pairs[p]
        enter = jnp.where(p > me, pair[1:2, :] + pair[0:1, :] * enter, enter)
    for h in range(heads):
        cols = slice(h * width, (h + 1) * width)
        state_grad = grad[:, cols] + prods[:, cols] * enter[:, cols]
        conv = conv_ref[:, cols].astype(jnp.float32)
        inp, norm = inp_ref[:, cols], norm_ref[:, cols]
        decays, reset = dec_ref[:, cols], reset_ref[:, cols]
        d_log = state_grad * decays * prev_ref[:, cols] - (
            state_grad * inp * conv * decays * decays / norm
        )
        d_r = (d_log * (-8.0 * slow_ref[:, cols]) * reset * (1.0 - reset)).astype(jnp.bfloat16)
        d_i = (state_grad * norm * conv * inp * (1.0 - inp)).astype(jnp.bfloat16)
        out_ref[:, cols] = (
            state_grad * norm * inp
            + lax.dot_general(d_r, wr_ref[h], (((1,), (1,)), ((), ())), preferred_element_type=jnp.float32)
            + lax.dot_general(d_i, wi_ref[h], (((1,), (1,)), ((), ())), preferred_element_type=jnp.float32)
        ).astype(jnp.bfloat16)
    keep.wait()
    for off in range(1, n):
        peer = lax.rem(me + off, n)
        block_to(peer, peer).wait_recv()
        block_to(peer, me).wait_send()


VM = pl.BlockSpec(memory_space=pltpu.VMEM)


def run_backward(n, *args):
    shape = args[2].shape
    half = jax.ShapeDtypeStruct(shape, jnp.bfloat16)
    return pl.pallas_call(
        functools.partial(backward_kernel, n),
        out_shape=(half, half, jax.ShapeDtypeStruct(args[-1].shape, jnp.bfloat16)),
        in_specs=[VM] * len(args),
        out_specs=(VM, VM, pl.BlockSpec(memory_space=pl.ANY)),
        scratch_shapes=[pltpu.VMEM(shape, jnp.float32)] * 3
        + [
            pltpu.VMEM((8, shape[1]), jnp.float32),
            pltpu.VMEM((n, 8, shape[1]), jnp.float32),
            pltpu.SemaphoreType.DMA((1,)),
            pltpu.SemaphoreType.DMA((n,)),
            pltpu.SemaphoreType.DMA((2,)),
            pltpu.SemaphoreType.DMA((n,)),
        ],
        compiler_params=pltpu.CompilerParams(collective_id=0, has_side_effects=True),
        cost_estimate=pl.CostEstimate(flops=400_000_000, bytes_accessed=40_000_000, transcendentals=0),
    )(*args)


def softplus_of_negative(x):
    small = jnp.exp(-jnp.abs(x))
    ratio = small / (2.0 + small)
    square = ratio * ratio
    series = jnp.zeros_like(x)
    for odd in range(17, 0, -2):
        series = series * square + 1.0 / odd
    return jnp.maximum(-x, 0.0) + 2.0 * ratio * series


def front_kernel(
    n, groups,
    mixed_ref, cot_ref, ids_ref, wts_ref,
    conv_ref, gate_ref, bs_ref, param_ref, shift_ref, wr_ref, wi_ref,
    wg_hbm, wu_hbm, wd_hbm,
    gg_hbm, gu_hbm, gd_hbm, dm_ref,
    merged_ref, slow_ref, reset_ref, inp_ref, dec_ref, norm_ref, st_ref, prev_ref,
    wg, wu, wd, send, xbuf, dbuf, hbuf, pbuf, nbuf, sbuf, fbuf, rbuf, ret, dcols, dmbuf,
    acc_g, acc_u, acc_d, drive,
    send_sem, sp_sem, y_sem, own_sem, fwd_sem, near_sem, far_sem, ret_sem, dm_sem, w_sem, g_sem,
):
    me, q = lax.axis_index("sp"), lax.axis_index("tp")
    near, far = q ^ 1, q ^ 2
    barrier = pltpu.get_barrier_semaphore()
    for off in range(1, n):
        pl.semaphore_signal(
            barrier, inc=1, device_id={"sp": lax.rem(me + off, n)}, device_id_type=MESH
        )
    for other in (near, far):
        pl.semaphore_signal(barrier, inc=1, device_id={"tp": other}, device_id_type=MESH)
    loads = [
        pltpu.make_async_copy(src, dst, w_sem.at[i])
        for i, (src, dst) in enumerate(((wg_hbm, wg), (wu_hbm, wu), (wd_hbm, wd)))
    ]
    for copy in loads:
        copy.start()
    tokens, width = mixed_ref.shape
    top = ids_ref.shape[1]
    slots = send.shape[2]
    hidden = wg.shape[1]
    parts = xbuf.shape[0]
    per = n // groups
    block = per * slots

    lanes = 128
    lane = lax.broadcasted_iota(jnp.int32, (tokens, lanes), 1)
    away = []
    for j in range(top):
        gap = ids_ref[:, j : j + 1] - me
        away.append(jnp.where(gap < 0, gap + n, gap))
    member = jnp.zeros((tokens, lanes), jnp.float32)
    for j in range(top):
        member = jnp.where(away[j] == lane, 1.0, member)
    earlier = lax.broadcasted_iota(jnp.int32, (tokens, tokens), 1) < (
        lax.broadcasted_iota(jnp.int32, (tokens, tokens), 0)
    )
    rank = jnp.dot(
        jnp.where(earlier, 1.0, 0.0).astype(jnp.bfloat16),
        member.astype(jnp.bfloat16),
        preferred_element_type=jnp.float32,
    )
    place = lax.broadcasted_iota(jnp.int32, (tokens, n * slots), 1)
    picks = []
    for j in range(top):
        mine = jnp.sum(jnp.where(away[j] == lane, rank, 0.0), axis=1, keepdims=True)
        at = away[j] * slots + mine.astype(jnp.int32)
        picks.append(jnp.where(place == at, 1.0, 0.0).astype(jnp.bfloat16))
    pick_all = picks[0]
    for j in range(1, top):
        pick_all = pick_all + picks[j]

    def over(left, right):
        return lax.dot_general(
            left, right, (((0,), (0,)), ((), ())), preferred_element_type=jnp.float32
        )

    def against(left, right):
        return lax.dot_general(
            left, right, (((1,), (1,)), ((), ())), preferred_element_type=jnp.float32
        )

    send[:, 0] = over(pick_all, mixed_ref[...]).astype(jnp.bfloat16).reshape(n, slots, width)
    chosen = jnp.zeros((n * slots, width), jnp.float32)
    for j in range(top):
        scaled = wts_ref[:, j : j + 1] * cot_ref[...].astype(jnp.float32)
        chosen = chosen + over(picks[j], scaled.astype(jnp.bfloat16))
    send[:, 1] = chosen.astype(jnp.bfloat16).reshape(n, slots, width)
    sent = []

    def remote(src, dst, recv, where):
        return pltpu.make_async_remote_copy(
            src_ref=src, dst_ref=dst, send_sem=send_sem.at[0], recv_sem=recv,
            device_id=where, device_id_type=MESH,
        )

    def start(copy):
        copy.start()
        sent.append(copy)

    def over_sp(k):
        return remote(
            send.at[k], xbuf.at[q, k], sp_sem.at[k], {"sp": lax.rem(me + k, n)}
        )

    def over_tp(owner, k, other, sems):
        spot = xbuf.at[owner, k]
        return remote(spot, spot, sems.at[k], {"tp": other})

    def spread(k):
        if k > 0:
            over_sp(k).wait_recv()
        start(over_tp(q, k, far, y_sem))
        start(over_tp(q, k, near, own_sem))

    def relay(k):
        over_tp(far, k, far, y_sem).wait_recv()
        start(over_tp(far, k, near, fwd_sem))

    def near_copy(g, i):
        return remote(
            pbuf.at[g, near if i == 0 else far ^ 1], nbuf.at[g, i], near_sem.at[g, i], {"tp": near}
        )

    def expert(g):
        ks = range(g * per, (g + 1) * per)
        for k in ks:
            over_tp(near, k, near, own_sem).wait_recv()
            over_tp(near ^ 2, k, near, fwd_sem).wait_recv()
        here = slice(g * per, (g + 1) * per)
        up_pre = jnp.zeros((block, hidden), jnp.float32)
        linear = jnp.zeros((block, hidden), jnp.float32)
        d_hidden = jnp.zeros((block, hidden), jnp.float32)
        for b in range(parts):
            cols = slice(b * width, (b + 1) * width)
            x = xbuf[b, here, 0].reshape(block, width)
            c = xbuf[b, here, 1].reshape(block, width)
            up_pre += jnp.dot(x, wg[cols, :], preferred_element_type=jnp.float32)
            linear += jnp.dot(x, wu[cols, :], preferred_element_type=jnp.float32)
            d_hidden += against(c, wd[:, cols])
        sig = jax.nn.sigmoid(up_pre)
        silu = up_pre * sig
        rows = slice(g * block, (g + 1) * block)
        hbuf[rows, :] = (silu * linear).astype(jnp.bfloat16)
        d_linear = (d_hidden * silu).astype(jnp.bfloat16)
        d_up = (d_hidden * linear * sig * (1.0 + up_pre * (1.0 - sig))).astype(jnp.bfloat16)
        dbuf[rows, :hidden] = d_up
        dbuf[rows, hidden:] = d_linear
        for b in range(parts):
            cols = slice(b * width, (b + 1) * width)
            pbuf[g, b] = (against(d_up, wg[cols, :]) + against(d_linear, wu[cols, :])).astype(
                jnp.bfloat16
            )
        for i in range(2):
            start(near_copy(g, 1 - i))

    def far_copy(g):
        return remote(sbuf.at[g], fbuf.at[g], far_sem.at[g], {"tp": far})

    def join_near(g):
        near_copy(g, 1).wait_recv()
        sbuf[g] = (pbuf[g, far].astype(jnp.float32) + nbuf[g, 1].astype(jnp.float32)).astype(
            jnp.bfloat16
        )
        start(far_copy(g))

    def back_copy(g, i):
        k = g * per + i
        return remote(
            rbuf.at[g, i], ret.at[k], ret_sem.at[k], {"sp": lax.rem(me + n - k, n)}
        )

    def join_far(g):
        near_copy(g, 0).wait_recv()
        far_copy(g).wait_recv()
        whole = (
            pbuf[g, q].astype(jnp.float32)
            + nbuf[g, 0].astype(jnp.float32)
            + fbuf[g].astype(jnp.float32)
        )
        rbuf[g] = whole.astype(jnp.bfloat16).reshape(per, slots, width)
        for i in range(per):
            if g * per + i > 0:
                start(back_copy(g, i))
        if g == 0:
            ret[0] = whole[:slots].astype(jnp.bfloat16)

    g_copies = []

    def grads(h):
        half = n // 2
        here = slice(h * half, (h + 1) * half)
        rows = slice(h * half * slots, (h + 1) * half * slots)
        d_both = dbuf[rows, :]
        hid = hbuf[rows, :]
        for b in range(parts):
            cols = slice(b * width, (b + 1) * width)
            x = xbuf[b, here, 0].reshape(half * slots, width)
            c = xbuf[b, here, 1].reshape(half * slots, width)
            both = over(x, d_both)
            down = over(hid, c)
            if h == 0:
                acc_g[cols, :] = both[:, :hidden]
                acc_u[cols, :] = both[:, hidden:]
                acc_d[:, cols] = down
            else:
                acc_g[cols, :] += both[:, :hidden]
                acc_u[cols, :] += both[:, hidden:]
                acc_d[:, cols] += down
        if h == 1:
            for i, (src, dst) in enumerate(((acc_g, gg_hbm), (acc_u, gu_hbm), (acc_d, gd_hbm))):
                copy = pltpu.make_async_copy(src, dst, g_sem.at[i])
                copy.start()
                g_copies.append(copy)

    pl.semaphore_wait(barrier, n + 1)
    for k in range(1, n):
        start(over_sp(k))
    xbuf[q, 0] = send[0]
    spread(0)
    slow = softplus_of_negative(param_ref[...])
    slow_ref[...] = slow
    eye = lax.broadcasted_iota(jnp.int32, (tokens, tokens), 0) == (
        lax.broadcasted_iota(jnp.int32, (tokens, tokens), 1)
    )
    shift = jnp.sum(jnp.where(eye, shift_ref[...], 0.0), axis=1, keepdims=True)
    recurrence_forward(
        conv_ref, gate_ref, bs_ref, slow, shift, wr_ref, wi_ref,
        merged_ref, reset_ref, inp_ref, dec_ref, norm_ref, st_ref, prev_ref, drive,
    )
    for copy in loads:
        copy.wait()
    done = 0
    for k in range(1, n + 1):
        if k < n:
            spread(k)
        relay(k - 1)
        ready = (k - 1) // per
        if k >= per + 1 and (k - 1) % per == 0:
            g = ready - 1
            expert(g)
            if g >= 1:
                join_near(g - 1)
            if g >= 2:
                join_far(g - 2)
            if g == groups // 2 - 1:
                pass
    last = groups - 1
    expert(last)
    join_near(last - 1)
    join_far(last - 2)
    join_near(last)
    grads(0)
    join_far(last - 1)
    join_far(last)
    grads(1)
    for k in range(1, n):
        back_copy(k // per, k % per).wait_recv()
    summed = jnp.dot(
        pick_all, ret[...].reshape(n * slots, width), preferred_element_type=jnp.float32
    )
    dcols[...] = (cot_ref[...].astype(jnp.float32) + summed).astype(jnp.bfloat16)

    def dm_copy(owner, i, other, src):
        return remote(src, dmbuf.at[owner], dm_sem.at[i], {"tp": other})

    start(dm_copy(q, 0, far, dcols))
    start(dm_copy(q, 1, near, dcols))
    dmbuf[q] = dcols[...]
    dm_copy(far, 0, far, dcols).wait_recv()
    start(dm_copy(far, 2, near, dmbuf.at[far]))
    dm_copy(near, 1, near, dcols).wait_recv()
    dm_copy(near ^ 2, 2, near, dcols).wait_recv()
    for b in range(parts):
        dm_ref[:, b * width : (b + 1) * width] = dmbuf[b]
    for copy in g_copies:
        copy.wait()
    for copy in sent:
        copy.wait_send()


def run_front(n, parts, slots, mixed, cot, ids, weights, conv, gate, bs, param, shift, wr, wi, wg, wu, wd):
    tokens, width = mixed.shape
    full, hidden = wg.shape
    groups = 4
    per = n // groups
    block = per * slots
    half = jnp.bfloat16
    anywhere = pl.BlockSpec(memory_space=pl.ANY)
    dma = pltpu.SemaphoreType.DMA
    f32 = jnp.float32
    wide = jax.ShapeDtypeStruct((tokens, width), f32)
    vm = pltpu.VMEM
    return pl.pallas_call(
        functools.partial(front_kernel, n, groups),
        out_shape=(
            jax.ShapeDtypeStruct((full, hidden), f32),
            jax.ShapeDtypeStruct((full, hidden), f32),
            jax.ShapeDtypeStruct((hidden, full), f32),
            jax.ShapeDtypeStruct((tokens, full), half),
            jax.ShapeDtypeStruct((tokens, width), half),
            jax.ShapeDtypeStruct((1, width), f32),
        ) + (wide,) * 6,
        in_specs=[VM] * 11 + [anywhere] * 3,
        out_specs=(anywhere,) * 3 + (VM,) * 9,
        scratch_shapes=[
            vm((full, hidden), half), vm((full, hidden), half), vm((hidden, full), half),
            vm((n, 2, slots, width), half),
            vm((parts, n, 2, slots, width), half),
            vm((n * slots, 2 * hidden), half), vm((n * slots, hidden), half),
            vm((groups, parts, block, width), half),
            vm((groups, 2, block, width), half),
            vm((groups, block, width), half),
            vm((groups, block, width), half),
            vm((groups, per, slots, width), half),
            vm((n, slots, width), half),
            vm((tokens, width), half),
            vm((parts, tokens, width), half),
            vm((full, hidden), f32), vm((full, hidden), f32), vm((hidden, full), f32),
            vm((tokens, width), f32),
            dma((1,)), dma((n,)), dma((n,)), dma((n,)), dma((n,)), dma((groups, 2)),
            dma((groups,)), dma((n,)), dma((3,)), dma((3,)), dma((3,)),
        ],
        compiler_params=pltpu.CompilerParams(
            collective_id=1, has_side_effects=True, vmem_limit_bytes=60 * 1024 * 1024
        ),
        cost_estimate=pl.CostEstimate(flops=8_000_000_000, bytes_accessed=80_000_000, transcendentals=0),
    )(mixed, cot, ids, weights, conv, gate, bs, param, shift, wr, wi, wg, wu, wd)


def over_rows(left_matrix, right_matrix):
    return lax.dot_general(
        left_matrix, right_matrix, (((0,), (0,)), ((), ())), preferred_element_type=jnp.float32
    )


def body(
    conv_out, gate_in, block_states, decay_param, decay_shift, w_reset, w_input, w_out,
    mixed, d_out, expert_ids, route_weights, w_gate, w_up, w_down,
):
    tok_rows, top_k = expert_ids.shape
    experts = lax.axis_size("sp")
    capacity = 2 * tok_rows * top_k // experts
    slots = -(-capacity // 16) * 16
    (
        grad_gate_e, grad_up_e, grad_down_e, d_mixed,
        merged_in, slow_rate, reset, input_gate, decays, norm_in, states, prev_states,
    ) = run_front(
        experts, lax.axis_size("tp"), slots, mixed, d_out, expert_ids, route_weights,
        conv_out, gate_in, block_states, decay_param[None, :], decay_shift[None, :],
        w_reset, w_input, w_gate[0], w_up[0], w_down[0],
    )
    merged_full = lax.all_gather(merged_in, "sp", axis=0, tiled=True)
    blocks = d_mixed.reshape(tok_rows, experts, -1).transpose(1, 0, 2)
    recurrence_input_gradient, grad_gate, got_blocks = run_backward(
        experts, d_mixed, w_out, conv_out, gate_in, slow_rate, reset, input_gate, decays, norm_in,
        states, prev_states, w_reset, w_input, blocks,
    )
    grad_out_proj_t = over_rows(got_blocks.reshape(experts * tok_rows, -1), merged_full)
    return (
        grad_gate_e[None],
        grad_up_e[None],
        grad_down_e[None],
        grad_out_proj_t,
        recurrence_input_gradient,
        grad_gate,
    )


def solution(mesh):
    placed = (
        P("sp", "tp"),
        P("sp", "tp"),
        P("sp", "tp"),
        P("tp"),
        P("sp"),
        P("tp", None, None),
        P("tp", None, None),
        P("tp", None),
        P("sp", "tp"),
        P("sp", "tp"),
        P("sp", None),
        P("sp", None),
        P("sp", None, "tp"),
        P("sp", None, "tp"),
        P("sp", "tp", None),
    )
    return jax.shard_map(
        body,
        mesh=mesh,
        in_specs=placed,
        out_specs=(
            P("sp", None, "tp"),
            P("sp", None, "tp"),
            P("sp", "tp", None),
            P("sp", "tp"),
            P("sp", "tp"),
            P("sp", "tp"),
        ),
        check_vma=False,
    )
```

time: 218 us -> 178 us (0.82)
  waiting for transfers between devices: 57.6 us -> 16.7 us
  Pallas kernels: 97.5 us -> 132 us
  matrix products: 20.7 us -> 3.04 us
  blocking collectives: 7.66 us -> 0 us
  starting transfers between devices: 5.54 us -> 0.04 us
  other arithmetic: 3.36 us -> 0 us
    reduce_scatter x1 -> x0, waiting for transfers between devices: 46.8 us -> none  [body(): lax.psum_scatter(partial_value.astype(jnp.bfloat16), 'tp', scatter_dimens...]
    pallas_call x2 -> x1, Pallas kernels: 68.9 us -> 98.6 us  [run_front(): pl.pallas_call(functools.partial(front_kernel, n, groups), out_shape=(jax...]
    all_gather x0 -> x1, waiting for transfers between devices: none -> 16.7 us  [body(): merged_full = lax.all_gather(merged_in, 'sp', axis=0, tiled=True)]
    all_to_all x1 -> x0, waiting for transfers between devices: 10.8 us -> none  [body(): lax.all_to_all(row_grad.reshape(experts, slots, columns), 'sp', split_axi...]
    dot_general x5 -> x0, matrix products: 9 us -> none  [the longest x3 4.99 us: against_rows(): lax.dot_general(left_matrix, right_matrix, (((1,), (1,)), ((), ())), pref...]
    dot_general x4 -> x1, matrix products: 11.7 us -> 3.04 us  [over_rows(): lax.dot_general(left_matrix, right_matrix, (((0,), (0,)), ((), ())), pref...]
    all_gather x1 -> x0, blocking collectives: 7.66 us -> none  [body(): d_mixed = lax.all_gather(d_columns, 'tp', axis=1, tiled=True)]
    all_to_all x1 -> x0, starting transfers between devices: 5.51 us -> none  [body(): lax.all_to_all(row_grad.reshape(experts, slots, columns), 'sp', split_axi...]
  transfers between devices with their start and end apart: 2 -> 1, of which waited for: 2 -> 1; matrix products, arithmetic and copies ran while one was open for 5% -> 1% of each run, Pallas kernels for 0% -> 19%
where the time goes in v1:
time: 178 us
  Pallas kernels  132 us (74%)
  waiting for transfers between devices  16.7 us (9%)
  between operations  14.1 us (8%)
  local copies, waits for them, and re-layouts  12.3 us (7%)
  matrix products  3.04 us (2%)
    pallas_call x1, Pallas kernels, run_front(): pl.pallas_call(functools.partial(front_kernel, n, groups), out_shape=(jax...  98.6 us
    pallas_call x1, Pallas kernels, run_backward(): pl.pallas_call(functools.partial(backward_kernel, n), out_shape=(half, ha...  33.4 us
    all_gather x1, waiting for transfers between devices, body(): merged_full = lax.all_gather(merged_in, 'sp', axis=0, tiled=True)  16.7 us
    unnamed x17, local copies, waits for them, and re-layouts  10.3 us
  transfers between devices with their start and end apart: 1, of which 1 were waited for; matrix products, arithmetic and copies ran while one was open for 1% of the time, Pallas kernels for 19%

profile of v1, /device:TPU:0, one launch (start us, length us, event | category | flops | bytes accessed | tf_op | source)
XLA Modules:
  0.0 178.1 jit_solution(5794333587273723070)
XLA Ops:
  7.2 0.0 all-gather.2.cloned.1.call-start
  7.2 1.4 copy.23.ids_ref
  8.7 1.4 copy.24.wts_ref
  10.1 98.6 %shard_map.190 = (f32[2048,256]{1,0:T(8,128)}, f32[2048,256]{1,0:T(8,128)}, f32[256,2048]{1,0:T(8,128)}, bf16[192,2048]{1,0:T(8,128)(2,1)}, bf16[192,512]{1,0:T(...) custom-call(bf16[192,512]{1,0:T(8,128)(2,1)} %mixed_ref.1, ...), custom_call_target="tpu_custom_call" | custom-call | flops 8000000000 | bytes 80000000 | tf_op jit(solution)/shard_map/pallas_call | solution.py:488
  108.7 0.0 all-gather.2.cloned.1.call-update
  108.7 2.1 %copy.28 = bf16[24,8,8,256]{3,2,0,1:T(8,128)(2,1)} copy(bf16[24,8,8,256]{3,2,1,0:T(8,128)(2,1)} %bitcast.18) | data formatting | bytes 1572864 | tf_op jit(solution)/shard_map/reshape | solution.py:548
  110.8 33.4 %shard_map.191 = (bf16[192,512]{1,0:T(8,128)(2,1)}, bf16[192,512]{1,0:T(8,128)(2,1)}, bf16[8,192,256]{2,1,0:T(8,128)(2,1)}) custom-call(bf16[192,2048]{1,0:T(8,128)(2,1)} %get-tuple-element.24.dm_ref, bf16[512,2048]{1,0:T(8,128)(2,1)} %wo_ref.1, bf16[192,512]{1,0:T(8,128)(2,1)} %conv_ref.3, bf16[192,512]{1,0:T(8,128)(2,1)} %gate_ref.3, ...), custom_call_target="tpu_custom_call" | custom-call | flops 400000000 | bytes 40000000 | tf_op jit(solution)/shard_map/pallas_call | solution.py:177
  144.2 0.0 copy-start.2
  144.2 16.7 %all-gather.2.cloned.1.call-done = bf16[1536,512]{1,0:T(8,128)(2,1)} async-done(((bf16[192,512]{1,0:T(8,128)(2,1)}), bf16[1536,512]{1,0:T(8,128)(2,1)}) %all-gather.2.cloned.1.call-update) | async-done | bytes 1572880 | tf_op jit(solution)/shard_map/all_gather | solution.py:547
  160.9 3.0 %fusion = f32[256,512]{1,0:T(8,128)} fusion(bf16[1536,256]{1,0:T(8,128)(2,1)} %bitcast.23, bf16[1536,512]{1,0:T(8,128)(2,1)} %all-gather.2.cloned.1.call-done), kind=kOutput, calls=%fused_computation.1 | convolution fusion | flops 402653184 | bytes 2883584 | tf_op jit(solution)/shard_map/dot_general | solution.py:526
  163.9 0.0 copy-done.2
  163.9 0.0 copy-start.1
  163.9 1.3 copy.34
  165.2 1.0 copy-done.1
  166.3 0.0 copy-start
  166.3 1.3 copy.35
  167.6 1.0 copy-done
  168.6 0.0 copy-start.4
  168.6 0.0 copy-start.3
  168.6 1.3 copy.36
  169.9 0.0 copy-done.4
  169.9 0.7 copy.37
  170.6 0.0 copy-done.3
  170.6 0.7 copy.38
Async XLA Ops:
  7.2 153.7 %all-gather.2.cloned.1.call-start = ((), (), s32[]{:S(2)}) async-start(), calls=%async_computation | async-start | bytes 1769472 | tf_op jit(solution)/shard_map/all_gather | solution.py:547
  144.2 19.7 %copy-start.2 = (f32[2048,256]{1,0:T(8,128)S(1)}, f32[2048,256]{1,0:T(8,128)}, u32[]{:S(2)}) copy-start(f32[2048,256]{1,0:T(8,128)} %get-tuple-element.21) | copy-start | bytes 6291460
  163.9 2.3 %copy-start.1 = (f32[2048,256]{1,0:T(8,128)S(1)}, f32[2048,256]{1,0:T(8,128)}, u32[]{:S(2)}) copy-start(f32[2048,256]{1,0:T(8,128)} %get-tuple-element.22) | copy-start | bytes 6291460
  166.3 2.3 %copy-start = (f32[256,2048]{1,0:T(8,128)S(1)}, f32[256,2048]{1,0:T(8,128)}, u32[]{:S(2)}) copy-start(f32[256,2048]{1,0:T(8,128)} %get-tuple-element.23) | copy-start | bytes 6291460
  168.6 1.3 copy-start.4
  168.6 2.0 %copy-start.3 = (bf16[192,512]{1,0:T(8,128)(2,1)S(1)}, bf16[192,512]{1,0:T(8,128)(2,1)}, u32[]{:S(2)}) copy-start(bf16[192,512]{1,0:T(8,128)(2,1)} %get-tuple-element.47) | copy-start | bytes 589828
Sparse Core Ops, SparseCore 0:
  108.9 51.9 all-gather.1

commit v2 on v1

v2 whole, which is shorter than its diff:
```python
import functools
import jax
import jax.numpy as jnp
from jax import lax
from jax.experimental import pallas as pl
from jax.experimental.pallas import tpu as pltpu
from jax.sharding import PartitionSpec as P

MESH = pl.DeviceIdType.MESH
GELU_C = 0.7978845608028654
GELU_K = 0.044715


def gelu_both(x):
    inner = jnp.tanh(GELU_C * (x + GELU_K * x * x * x))
    act = 0.5 * x * (1.0 + inner)
    slope = 0.5 * (1.0 + inner) + 0.5 * x * (1.0 - inner * inner) * (
        GELU_C * (1.0 + 3.0 * GELU_K * x * x)
    )
    return act, slope


def softplus_of_negative(x):
    small = jnp.exp(-jnp.abs(x))
    ratio = small / (2.0 + small)
    square = ratio * ratio
    series = jnp.zeros_like(x)
    for odd in range(17, 0, -2):
        series = series * square + 1.0 / odd
    return jnp.maximum(-x, 0.0) + 2.0 * ratio * series


def whole_kernel(
    n, groups,
    mixed_ref, cot_ref, ids_ref, wts_ref,
    conv_ref, gate_ref, bs_ref, param_ref, shift_ref, wr_ref, wi_ref,
    wg_hbm, wu_hbm, wd_hbm, wo_hbm,
    gg_hbm, gu_hbm, gd_hbm, go_ref, out_ref, gate_out_ref,
    wg, wu, wd, wo, send, xbuf, dbuf, hbuf, pbuf, nbuf, sbuf, fbuf, rbuf, ret, dcols, dmbuf,
    acc_g, acc_u, acc_d, dec, drive, st, act_b, slope_b, fac_r, fac_i, fac_o, prods, lev0, lev1, lev2, grad,
    mg, got, bsend, mine_pair, pairs,
    send_sem, sp_sem, y_sem, own_sem, fwd_sem, near_sem, far_sem, ret_sem, dm_sem, w_sem, g_sem,
    mz_sem, mx_sem, blk_sem, got_sem, pair_sem,
):
    me, q = lax.axis_index("sp"), lax.axis_index("tp")
    near, far = q ^ 1, q ^ 2
    barrier = pltpu.get_barrier_semaphore()
    for off in range(1, n):
        pl.semaphore_signal(
            barrier, inc=1, device_id={"sp": lax.rem(me + off, n)}, device_id_type=MESH
        )
    for other in (near, far):
        pl.semaphore_signal(barrier, inc=1, device_id={"tp": other}, device_id_type=MESH)
    loads = [
        pltpu.make_async_copy(src, dst, w_sem.at[i])
        for i, (src, dst) in enumerate(((wg_hbm, wg), (wu_hbm, wu), (wd_hbm, wd), (wo_hbm, wo)))
    ]
    for copy in loads:
        copy.start()
    tokens, width = mixed_ref.shape
    top = ids_ref.shape[0]
    slots = send.shape[2]
    hidden = wg.shape[1]
    parts = xbuf.shape[0]
    per = n // groups
    block = per * slots
    heads, head_dim = wr_ref.shape[0], wr_ref.shape[1]
    f32, half = jnp.float32, jnp.bfloat16

    eye = lax.broadcasted_iota(jnp.int32, (tokens, tokens), 0) == (
        lax.broadcasted_iota(jnp.int32, (tokens, tokens), 1)
    )

    def upright(row):
        return jnp.sum(jnp.where(eye, row, jnp.zeros_like(row)), axis=1, keepdims=True)

    lanes = 128
    lane = lax.broadcasted_iota(jnp.int32, (tokens, lanes), 1)
    away = []
    for j in range(top):
        gap = upright(ids_ref[j : j + 1, :].astype(f32)).astype(jnp.int32) - me
        away.append(jnp.where(gap < 0, gap + n, gap))
    member = jnp.zeros((tokens, lanes), f32)
    for j in range(top):
        member = jnp.where(away[j] == lane, 1.0, member)
    earlier = lax.broadcasted_iota(jnp.int32, (tokens, tokens), 1) < (
        lax.broadcasted_iota(jnp.int32, (tokens, tokens), 0)
    )
    rank = jnp.dot(
        jnp.where(earlier, 1.0, 0.0).astype(half), member.astype(half), preferred_element_type=f32
    )
    place = lax.broadcasted_iota(jnp.int32, (tokens, n * slots), 1)
    picks = []
    for j in range(top):
        mine = jnp.sum(jnp.where(away[j] == lane, rank, 0.0), axis=1, keepdims=True)
        at = away[j] * slots + mine.astype(jnp.int32)
        picks.append(jnp.where(place == at, 1.0, 0.0).astype(half))
    pick_all = picks[0]
    for j in range(1, top):
        pick_all = pick_all + picks[j]

    def over(left, right):
        return lax.dot_general(left, right, (((0,), (0,)), ((), ())), preferred_element_type=f32)

    def against(left, right):
        return lax.dot_general(left, right, (((1,), (1,)), ((), ())), preferred_element_type=f32)

    send[:, 0] = over(pick_all, mixed_ref[...]).astype(half).reshape(n, slots, width)
    chosen = jnp.zeros((n * slots, width), f32)
    for j in range(top):
        scaled = upright(wts_ref[j : j + 1, :]) * cot_ref[...].astype(f32)
        chosen = chosen + over(picks[j], scaled.astype(half))
    send[:, 1] = chosen.astype(half).reshape(n, slots, width)
    sent = []

    def remote(src, dst, recv, where):
        return pltpu.make_async_remote_copy(
            src_ref=src, dst_ref=dst, send_sem=send_sem.at[0], recv_sem=recv,
            device_id=where, device_id_type=MESH,
        )

    def start(copy):
        copy.start()
        sent.append(copy)

    def over_sp(k):
        return remote(send.at[k], xbuf.at[q, k], sp_sem.at[k], {"sp": lax.rem(me + k, n)})

    def over_tp(owner, k, other, sems):
        spot = xbuf.at[owner, k]
        return remote(spot, spot, sems.at[k], {"tp": other})

    def spread(k):
        if k > 0:
            over_sp(k).wait_recv()
        start(over_tp(q, k, far, y_sem))
        start(over_tp(q, k, near, own_sem))

    def relay(k):
        over_tp(far, k, far, y_sem).wait_recv()
        start(over_tp(far, k, near, fwd_sem))

    def near_copy(g, i):
        return remote(
            pbuf.at[g, near if i == 0 else far ^ 1], nbuf.at[g, i], near_sem.at[g, i], {"tp": near}
        )

    def expert(g):
        for k in range(g * per, (g + 1) * per):
            over_tp(near, k, near, own_sem).wait_recv()
            over_tp(near ^ 2, k, near, fwd_sem).wait_recv()
        here = slice(g * per, (g + 1) * per)
        up_pre = jnp.zeros((block, hidden), f32)
        linear = jnp.zeros((block, hidden), f32)
        d_hidden = jnp.zeros((block, hidden), f32)
        for b in range(parts):
            cols = slice(b * width, (b + 1) * width)
            x = xbuf[b, here, 0].reshape(block, width)
            c = xbuf[b, here, 1].reshape(block, width)
            up_pre += jnp.dot(x, wg[cols, :], preferred_element_type=f32)
            linear += jnp.dot(x, wu[cols, :], preferred_element_type=f32)
            d_hidden += against(c, wd[:, cols])
        sig = jax.nn.sigmoid(up_pre)
        silu = up_pre * sig
        rows = slice(g * block, (g + 1) * block)
        hbuf[rows, :] = (silu * linear).astype(half)
        d_linear = (d_hidden * silu).astype(half)
        d_up = (d_hidden * linear * sig * (1.0 + up_pre * (1.0 - sig))).astype(half)
        dbuf[rows, :hidden] = d_up
        dbuf[rows, hidden:] = d_linear
        for b in range(parts):
            cols = slice(b * width, (b + 1) * width)
            pbuf[g, b] = (against(d_up, wg[cols, :]) + against(d_linear, wu[cols, :])).astype(half)
        for i in range(2):
            start(near_copy(g, 1 - i))

    def far_copy(g):
        return remote(sbuf.at[g], fbuf.at[g], far_sem.at[g], {"tp": far})

    def join_near(g):
        near_copy(g, 1).wait_recv()
        sbuf[g] = (pbuf[g, far].astype(f32) + nbuf[g, 1].astype(f32)).astype(half)
        start(far_copy(g))

    def back_copy(g, i):
        k = g * per + i
        return remote(
            rbuf.at[g, i], ret.at[k], ret_sem.at[k], {"sp": lax.rem(me + n - k, n)}
        )

    def join_far(g):
        near_copy(g, 0).wait_recv()
        far_copy(g).wait_recv()
        whole = pbuf[g, q].astype(f32) + nbuf[g, 0].astype(f32) + fbuf[g].astype(f32)
        rbuf[g] = whole.astype(half).reshape(per, slots, width)
        for i in range(per):
            if g * per + i > 0:
                start(back_copy(g, i))
        if g == 0:
            ret[0] = whole[:slots].astype(half)

    def grads(h, b):
        some = n // 2
        here = slice(h * some, (h + 1) * some)
        rows = slice(h * some * slots, (h + 1) * some * slots)
        cols = slice(b * width, (b + 1) * width)
        both = over(xbuf[b, here, 0].reshape(some * slots, width), dbuf[rows, :])
        down = over(hbuf[rows, :], xbuf[b, here, 1].reshape(some * slots, width))
        if h == 0:
            acc_g[cols, :] = both[:, :hidden]
            acc_u[cols, :] = both[:, hidden:]
            acc_d[:, cols] = down
        else:
            acc_g[cols, :] += both[:, :hidden]
            acc_u[cols, :] += both[:, hidden:]
            acc_d[:, cols] += down

    lines = n // 2

    def ring_source(j):
        return lax.rem(me + n - 2 * j, n)

    def ring_send(j, source):
        start(remote(mg.at[source], mg.at[source], mx_sem.at[j], {"sp": me ^ 1}))
        if j < lines - 1:
            start(remote(mg.at[source], mg.at[source], mz_sem.at[j + 1], {"sp": lax.rem(me + 2, n)}))

    def ring(j):
        source = ring_source(j)
        spot = mg.at[source]
        if j > 0:
            remote(spot, spot, mz_sem.at[j], {"sp": me ^ 1}).wait_recv()
        ring_send(j, source)

    pl.semaphore_wait(barrier, n + 1)
    for k in range(1, n):
        start(over_sp(k))
    xbuf[q, 0] = send[0]
    spread(0)

    total = width
    row = lax.broadcasted_iota(jnp.int32, (8, total), 0)

    def forward():
        slow = softplus_of_negative(param_ref[...])
        shift = upright(shift_ref[...])
        for h in range(heads):
            cols = slice(h * head_dim, (h + 1) * head_dim)
            conv = conv_ref[:, cols]
            reset = jax.nn.sigmoid(jnp.dot(conv, wr_ref[h], preferred_element_type=f32))
            inp = jax.nn.sigmoid(jnp.dot(conv, wi_ref[h], preferred_element_type=f32))
            log_decay = -8.0 * reset * slow[:, cols] + shift
            decays = jnp.exp(log_decay)
            norm = jnp.sqrt(-jnp.tanh(log_decay) * (decays * decays + 1.0))
            conv = conv.astype(f32)
            dec[:, cols] = decays
            drive[:, cols] = norm * inp * conv
            fac_o[:, cols] = norm * inp
            fac_i[:, cols] = norm * conv * inp * (1.0 - inp)
            fac_r[:, cols] = (-8.0 * slow[:, cols]) * reset * (1.0 - reset)
            grad[:, cols] = inp * conv * decays * decays / norm

    def forward_scan():
        carry = bs_ref[...]
        for i in range(tokens // 8):
            at = slice(8 * i, 8 * i + 8)
            decay = dec[at, :]
            a = decay
            b = drive[at, :]
            for d in (1, 2, 4):
                b = b + a * jnp.where(row >= d, pltpu.roll(b, d, 0), 0.0)
                a = a * jnp.where(row >= d, pltpu.roll(a, d, 0), 1.0)
            state = a * carry + b
            st[at, :] = state
            prev = jnp.where(row >= 1, pltpu.roll(state, 1, 0), carry)
            fac_r[at, :] = fac_r[at, :] * (decay * prev - grad[at, :])
            carry = state[7:8, :]

    def forward_gate():
        for h in range(heads):
            cols = slice(h * head_dim, (h + 1) * head_dim)
            act, slope = gelu_both(gate_ref[:, cols].astype(f32))
            mg[me, :, cols] = (act * st[:, cols]).astype(half)
            act_b[:, cols] = act
            slope_b[:, cols] = st[:, cols] * slope

    def back_products():
        carry_p = jnp.ones((1, total), f32)
        following = jnp.ones((1, total), f32)
        for i in reversed(range(tokens // 8)):
            at = slice(8 * i, 8 * i + 8)
            decay = dec[at, :]
            a = jnp.where(row < 7, pltpu.roll(decay, 7, 0), following)
            following = decay[0:1, :]
            for d, level in ((1, lev0), (2, lev1), (4, lev2)):
                level[at, :] = jnp.where(row < 8 - d, a, 0.0)
                a = a * jnp.where(row < 8 - d, pltpu.roll(a, 8 - d, 0), 1.0)
            drive[at, :] = a
            p = a * carry_p
            prods[at, :] = p
            carry_p = p[0:1, :]

    fillers = [forward, forward_scan, forward_gate, back_products]
    for fill in fillers[:3]:
        fill()
    late = [fillers[3]]
    for copy in loads:
        copy.wait()
    grad_chunks = [functools.partial(grads, 0, b) for b in range(parts)]
    steps = [functools.partial(ring, j) for j in range(lines)]
    for k in range(1, n + 1):
        if k < n:
            spread(k)
        relay(k - 1)
        if k == 1:
            back_products()
        if k >= per + 1 and (k - 1) % per == 0:
            g = (k - 1) // per - 1
            expert(g)
            if g >= 1:
                join_near(g - 1)
            if g >= 2:
                join_far(g - 2)
        if k > 2 * per + 1 and (k - 1) % per != 0 and grad_chunks:
            grad_chunks.pop(0)()
        if k == n - 1:
            steps.pop(0)()
    last = groups - 1
    expert(last)
    join_near(last - 1)
    steps.pop(0)()
    join_far(last - 2)
    join_near(last)
    while grad_chunks:
        grad_chunks.pop(0)()
    join_far(last - 1)
    grads(1, 0)
    if steps:
        steps.pop(0)()
    join_far(last)
    for b in range(1, parts):
        grads(1, b)
    g_copies = []
    for i, (src, dst) in enumerate(((acc_g, gg_hbm), (acc_u, gu_hbm), (acc_d, gd_hbm))):
        copy = pltpu.make_async_copy(src, dst, g_sem.at[i])
        copy.start()
        g_copies.append(copy)
    for k in range(1, n):
        back_copy(k // per, k % per).wait_recv()
    summed = jnp.dot(pick_all, ret[...].reshape(n * slots, width), preferred_element_type=f32)
    dcols[...] = (cot_ref[...].astype(f32) + summed).astype(half)

    some = n // parts
    thin = width // some
    quarter = tokens // parts
    owner_q = lax.div(me, some)

    def blk_copy(i, x):
        peer, part = q * some + i, q ^ x
        at = pl.ds(pl.multiple_of(part * quarter, quarter), quarter)
        return pltpu.make_async_remote_copy(
            src_ref=bsend.at[i, at], dst_ref=got.at[me, at], send_sem=send_sem.at[1],
            recv_sem=blk_sem.at[me], device_id={"sp": peer, "tp": part}, device_id_type=MESH,
        )

    mine_at = pl.ds(pl.multiple_of(q * quarter, quarter), quarter)

    def blk_wait(source):
        spot = got.at[source, mine_at]
        remote(spot, spot, blk_sem.at[source], {"tp": far}).wait_recv()

    def dm_copy(owner, i, other, src):
        return remote(src, dmbuf.at[owner], dm_sem.at[i], {"tp": other})

    start(dm_copy(q, 0, far, dcols))
    start(dm_copy(q, 1, near, dcols))
    for i in range(some):
        bsend[i] = dcols[:, i * thin : (i + 1) * thin]
    for i in range(some):
        for x in range(1, parts):
            start(blk_copy(i, x))

        @pl.when(q * some + i != me)
        def _():
            blk_copy(i, 0).start()

        @pl.when(q * some + i == me)
        def _():
            got[me, mine_at] = bsend[i, mine_at]

    while steps:
        steps.pop(0)()
    dmbuf[q] = dcols[...]

    wo_cols = pl.ds(pl.multiple_of(q * width, width), width)
    grad[...] = against(dcols[...], wo[:, wo_cols])
    dm_copy(far, 0, far, dcols).wait_recv()
    start(dm_copy(far, 2, near, dmbuf.at[far]))
    dm_copy(near, 1, near, dcols).wait_recv()
    dm_copy(near ^ 2, 2, near, dcols).wait_recv()
    for shift_by in (1, 2, 3):
        other = q ^ shift_by
        at = pl.ds(pl.multiple_of(other * width, width), width)
        grad[...] += against(dmbuf[other], wo[:, at])
    for off in range(1, n):
        blk_wait(lax.rem(me + off, n))

    @pl.when(q != owner_q)
    def _():
        blk_wait(me)

    def got_copy(part, i, other):
        at = pl.ds(pl.multiple_of(part * quarter, quarter), quarter)
        spot = got.at[:, at]
        return remote(spot, spot, got_sem.at[i], {"tp": other})

    start(got_copy(q, 0, far))
    start(got_copy(q, 1, near))

    carry = jnp.zeros((1, total), f32)
    for i in reversed(range(tokens // 8)):
        at = slice(8 * i, 8 * i + 8)
        b = grad[at, :]
        gate_out_ref[at, :] = (b * slope_b[at, :]).astype(half)
        b = b * act_b[at, :]
        b = b + lev0[at, :] * pltpu.roll(b, 7, 0)
        b = b + lev1[at, :] * pltpu.roll(b, 6, 0)
        b = b + lev2[at, :] * pltpu.roll(b, 4, 0)
        g = drive[at, :] * carry + b
        grad[at, :] = g
        carry = g[0:1, :]
    first = dec[0:1, :]
    mine_pair[0:1, :] = prods[0:1, :] * first
    mine_pair[1:2, :] = carry * first
    mine_pair[2:8, :] = jnp.zeros((6, total), f32)
    pairs[me] = jnp.zeros((8, total), f32)

    def pair_to(peer, source):
        return remote(mine_pair, pairs.at[source], pair_sem.at[source], {"sp": peer})

    for off in range(1, n):
        start(pair_to(lax.rem(me + off, n), me))
    got_copy(far, 0, far).wait_recv()
    start(got_copy(far, 2, near))
    for off in range(1, n):
        peer = lax.rem(me + off, n)
        pair_to(peer, peer).wait_recv()
    enter = jnp.zeros((1, total), f32)
    for p in reversed(range(n)):
        pair = pairs[p]
        enter = jnp.where(p > me, pair[1:2, :] + pair[0:1, :] * enter, enter)
    for h in range(heads):
        cols = slice(h * head_dim, (h + 1) * head_dim)
        g = grad[:, cols] + prods[:, cols] * enter[:, cols]
        d_r = (g * fac_r[:, cols]).astype(half)
        d_i = (g * fac_i[:, cols]).astype(half)
        out_ref[:, cols] = (
            g * fac_o[:, cols] + against(d_r, wr_ref[h]) + against(d_i, wi_ref[h])
        ).astype(half)
    for j in range(lines):
        spot = mg.at[ring_source(j) ^ 1]
        remote(spot, spot, mx_sem.at[j], {"sp": me ^ 1}).wait_recv()
    got_copy(near, 1, near).wait_recv()
    got_copy(near ^ 2, 2, near).wait_recv()
    go_ref[...] = over(got[...].reshape(n * tokens, thin), mg[...].reshape(n * tokens, width))
    for copy in g_copies:
        copy.wait()
    for copy in sent:
        copy.wait_send()
    for i in range(some):

        @pl.when(q * some + i != me)
        def _():
            blk_copy(i, 0).wait_send()


VM = pl.BlockSpec(memory_space=pltpu.VMEM)


def run_whole(
    n, parts, slots, mixed, cot, ids, weights, conv, gate, bs, param, shift, wr, wi, wg, wu, wd, wo
):
    tokens, width = mixed.shape
    full, hidden = wg.shape
    groups = 4
    per = n // groups
    block = per * slots
    some = n // parts
    thin = width // some
    half, f32 = jnp.bfloat16, jnp.float32
    anywhere = pl.BlockSpec(memory_space=pl.ANY)
    dma, vm = pltpu.SemaphoreType.DMA, pltpu.VMEM
    shape = jax.ShapeDtypeStruct
    return pl.pallas_call(
        functools.partial(whole_kernel, n, groups),
        out_shape=(
            shape((full, hidden), f32), shape((full, hidden), f32), shape((hidden, full), f32),
            shape((thin, width), f32), shape((tokens, width), half), shape((tokens, width), half),
        ),
        in_specs=[VM] * 11 + [anywhere] * 4,
        out_specs=(anywhere,) * 3 + (VM,) * 3,
        scratch_shapes=[
            vm((full, hidden), half), vm((full, hidden), half), vm((hidden, full), half),
            vm((width, full), half),
            vm((n, 2, slots, width), half),
            vm((parts, n, 2, slots, width), half),
            vm((n * slots, 2 * hidden), half), vm((n * slots, hidden), half),
            vm((groups, parts, block, width), half),
            vm((groups, 2, block, width), half),
            vm((groups, block, width), half),
            vm((groups, block, width), half),
            vm((groups, per, slots, width), half),
            vm((n, slots, width), half),
            vm((tokens, width), half),
            vm((parts, tokens, width), half),
            vm((full, hidden), f32), vm((full, hidden), f32), vm((hidden, full), f32),
        ] + [vm((tokens, width), f32)] * 13 + [
            vm((n, tokens, width), half),
            vm((n, tokens, thin), half),
            vm((some, tokens, thin), half),
            vm((8, width), f32),
            vm((n, 8, width), f32),
            dma((2,)), dma((n,)), dma((n,)), dma((n,)), dma((n,)), dma((groups, 2)),
            dma((groups,)), dma((n,)), dma((3,)), dma((4,)), dma((3,)),
            dma((n // 2,)), dma((n // 2,)), dma((n,)), dma((3,)), dma((n,)),
        ],
        compiler_params=pltpu.CompilerParams(
            collective_id=0, has_side_effects=True, vmem_limit_bytes=63000 * 1024
        ),
        cost_estimate=pl.CostEstimate(flops=8_000_000_000, bytes_accessed=80_000_000, transcendentals=0),
    )(mixed, cot, ids, weights, conv, gate, bs, param, shift, wr, wi, wg, wu, wd, wo)


def body(
    conv_out, gate_in, block_states, decay_param, decay_shift, w_reset, w_input, w_out,
    mixed, d_out, expert_ids, route_weights, w_gate, w_up, w_down,
):
    tok_rows, top_k = expert_ids.shape
    experts = lax.axis_size("sp")
    capacity = 2 * tok_rows * top_k // experts
    slots = -(-capacity // 16) * 16
    grad_gate_e, grad_up_e, grad_down_e, grad_out, grad_in, grad_gate = run_whole(
        experts, lax.axis_size("tp"), slots, mixed, d_out, expert_ids.T, route_weights.T,
        conv_out, gate_in, block_states, decay_param[None, :], decay_shift[None, :],
        w_reset, w_input, w_gate[0], w_up[0], w_down[0], w_out,
    )
    return (grad_gate_e[None], grad_up_e[None], grad_down_e[None], grad_out, grad_in, grad_gate)


def solution(mesh):
    placed = (
        P("sp", "tp"),
        P("sp", "tp"),
        P("sp", "tp"),
        P("tp"),
        P("sp"),
        P("tp", None, None),
        P("tp", None, None),
        P("tp", None),
        P("sp", "tp"),
        P("sp", "tp"),
        P("sp", None),
        P("sp", None),
        P("sp", None, "tp"),
        P("sp", None, "tp"),
        P("sp", "tp", None),
    )
    return jax.shard_map(
        body,
        mesh=mesh,
        in_specs=placed,
        out_specs=(
            P("sp", None, "tp"),
            P("sp", None, "tp"),
            P("sp", "tp", None),
            P("sp", "tp"),
            P("sp", "tp"),
            P("sp", "tp"),
        ),
        check_vma=False,
    )
```

time: 178 us -> 128 us (0.72)
  waiting for transfers between devices: 16.7 us -> 0 us
  Pallas kernels: 132 us -> 118 us
  between operations: 14.1 us -> 0.66 us
  local copies, waits for them, and re-layouts: 12.3 us -> 9.07 us
  matrix products: 3.04 us -> 0 us
    all_gather x1 -> x0, waiting for transfers between devices: 16.7 us -> none  [body(): merged_full = lax.all_gather(merged_in, 'sp', axis=0, tiled=True)]
    pallas_call x2 -> x1, Pallas kernels: 132 us -> 118 us  [run_whole(): pl.pallas_call(functools.partial(whole_kernel, n, groups), out_shape=(sha...]
    dot_general x1 -> x0, matrix products: 3.04 us -> none  [over_rows(): lax.dot_general(left_matrix, right_matrix, (((0,), (0,)), ((), ())), pref...]
    reshape x1 -> x0, local copies, waits for them, and re-layouts: 2.06 us -> none  [body(): blocks = d_mixed.reshape(tok_rows, experts, -1).transpose(1, 0, 2)]
    unnamed x17 -> x16, local copies, waits for them, and re-layouts: 10.3 us -> 9.07 us
  transfers between devices with their start and end apart: 1 -> 0, of which waited for: 1 -> 0; matrix products, arithmetic and copies ran while one was open for 1% -> 0% of each run, Pallas kernels for 19% -> 0%
where the time goes in v2:
time: 128 us
  Pallas kernels  118 us (92%)
  local copies, waits for them, and re-layouts  9.07 us (7%)
    pallas_call x1, Pallas kernels, run_whole(): pl.pallas_call(functools.partial(whole_kernel, n, groups), out_shape=(sha...  118 us
    unnamed x16, local copies, waits for them, and re-layouts  9.07 us

profile of v2, /device:TPU:0, one launch (start us, length us, event | category | flops | bytes accessed | tf_op | source)
XLA Modules:
  0.0 127.9 jit_solution(15841358078931367727)
XLA Ops:
  0.6 118.1 %shard_map.190 = (f32[2048,256]{1,0:T(8,128)}, f32[2048,256]{1,0:T(8,128)}, f32[256,2048]{1,0:T(8,128)}, f32[256,512]{1,0:T(8,128)}, bf16[192,512]{1,0:T(8,128)(2,1)}, /*index=5*/bf16[192,512]{1,0:T(8,128)(2,1)}) custom-call(bf16[192,512]{1,0:T(8,128)(2,1)} %mixed_ref.1, bf16[192,512]{1,0:T(8,128)(2,1)} %cot_ref.1, s32[2,192]{1,0:T(2,128)} %bitcast.16, ...), custom_call_target="tpu_custom_call" | custom-call | flops 8000000000 | bytes 80000000 | tf_op jit(solution)/shard_map/pallas_call | solution.py:494
  118.8 0.0 copy-start.1
  118.8 3.2 %copy.27 = f32[1,2048,256]{2,1,0:T(8,128)} copy(f32[1,2048,256]{2,1,0:T(8,128)} %bitcast.12) | data formatting | bytes 4194304
  122.0 0.0 copy-done.1
  122.0 0.0 copy-start
  122.0 1.3 %copy.28 = f32[1,2048,256]{2,1,0:T(8,128)} copy(f32[1,2048,256]{2,1,0:T(8,128)S(1)} %bitcast.11) | data formatting | bytes 4194304
  123.3 1.0 copy-done
  124.3 0.0 copy-start.2
  124.3 0.0 copy-start.4
  124.3 0.0 copy-start.3
  124.3 1.3 %copy.29 = f32[1,256,2048]{2,1,0:T(8,128)} copy(f32[1,256,2048]{2,1,0:T(8,128)S(1)} %bitcast.10) | data formatting | bytes 4194304
  125.7 0.0 copy-done.2
  125.7 0.8 copy.30
  126.5 0.0 copy-done.4
  126.5 0.7 copy.31
  127.2 0.0 copy-done.3
  127.2 0.7 copy.32
Async XLA Ops:
  118.8 3.2 %copy-start.1 = (f32[2048,256]{1,0:T(8,128)S(1)}, f32[2048,256]{1,0:T(8,128)}, u32[]{:S(2)}) copy-start(f32[2048,256]{1,0:T(8,128)} %get-tuple-element.13) | copy-start | bytes 6291460
  122.0 2.3 %copy-start = (f32[256,2048]{1,0:T(8,128)S(1)}, f32[256,2048]{1,0:T(8,128)}, u32[]{:S(2)}) copy-start(f32[256,2048]{1,0:T(8,128)} %get-tuple-element.14) | copy-start | bytes 6291460
  124.3 1.4 %copy-start.2 = (f32[256,512]{1,0:T(8,128)S(1)}, f32[256,512]{1,0:T(8,128)}, u32[]{:S(2)}) copy-start(f32[256,512]{1,0:T(8,128)} %get-tuple-element.27) | copy-start | bytes 1572868
  124.3 2.2 %copy-start.4 = (bf16[192,512]{1,0:T(8,128)(2,1)S(1)}, bf16[192,512]{1,0:T(8,128)(2,1)}, u32[]{:S(2)}) copy-start(bf16[192,512]{1,0:T(8,128)(2,1)} %get-tuple-element.28) | copy-start | bytes 589828
  124.3 2.8 %copy-start.3 = (bf16[192,512]{1,0:T(8,128)(2,1)S(1)}, bf16[192,512]{1,0:T(8,128)(2,1)}, u32[]{:S(2)}) copy-start(bf16[192,512]{1,0:T(8,128)(2,1)} %get-tuple-element.29) | copy-start | bytes 589828

commit v3 on v2

--- a/solution.py
+++ b/solution.py
@@ -36,10 +36,10 @@
     conv_ref, gate_ref, bs_ref, param_ref, shift_ref, wr_ref, wi_ref,
     wg_hbm, wu_hbm, wd_hbm, wo_hbm,
     gg_hbm, gu_hbm, gd_hbm, go_ref, out_ref, gate_out_ref,
-    wg, wu, wd, wo, send, xbuf, dbuf, hbuf, pbuf, nbuf, sbuf, fbuf, rbuf, ret, dcols, dmbuf,
+    wg, wu, wd, wo, info, tok, send, xbuf, dbuf, hbuf, pbuf, nbuf, sbuf, fbuf, rbuf, ret, dcols, dmbuf,
     acc_g, acc_u, acc_d, dec, drive, st, act_b, slope_b, fac_r, fac_i, fac_o, prods, lev0, lev1, lev2, grad,
     mg, got, bsend, mine_pair, pairs,
-    send_sem, sp_sem, y_sem, own_sem, fwd_sem, near_sem, far_sem, ret_sem, dm_sem, w_sem, g_sem,
+    send_sem, tok_send, credit, tok_sem, info_sem, x_sem, y_sem, own_sem, fwd_sem, near_sem, far_sem, ret_sem, dm_sem, w_sem, g_sem,
     mz_sem, mx_sem, blk_sem, got_sem, pair_sem,
 ):
     me, q = lax.axis_index("sp"), lax.axis_index("tp")
@@ -74,30 +74,10 @@
     def upright(row):
         return jnp.sum(jnp.where(eye, row, jnp.zeros_like(row)), axis=1, keepdims=True)
 
-    lanes = 128
-    lane = lax.broadcasted_iota(jnp.int32, (tokens, lanes), 1)
-    away = []
     for j in range(top):
-        gap = upright(ids_ref[j : j + 1, :].astype(f32)).astype(jnp.int32) - me
-        away.append(jnp.where(gap < 0, gap + n, gap))
-    member = jnp.zeros((tokens, lanes), f32)
-    for j in range(top):
-        member = jnp.where(away[j] == lane, 1.0, member)
-    earlier = lax.broadcasted_iota(jnp.int32, (tokens, tokens), 1) < (
-        lax.broadcasted_iota(jnp.int32, (tokens, tokens), 0)
-    )
-    rank = jnp.dot(
-        jnp.where(earlier, 1.0, 0.0).astype(half), member.astype(half), preferred_element_type=f32
-    )
-    place = lax.broadcasted_iota(jnp.int32, (tokens, n * slots), 1)
-    picks = []
-    for j in range(top):
-        mine = jnp.sum(jnp.where(away[j] == lane, rank, 0.0), axis=1, keepdims=True)
-        at = away[j] * slots + mine.astype(jnp.int32)
-        picks.append(jnp.where(place == at, 1.0, 0.0).astype(half))
-    pick_all = picks[0]
-    for j in range(1, top):
-        pick_all = pick_all + picks[j]
+        info[0, j : j + 1, :] = ids_ref[j : j + 1, :].astype(f32)
+        info[0, top + j : top + j + 1, :] = wts_ref[j : j + 1, :]
+    info[0, 2 * top :, :] = jnp.zeros((info.shape[1] - 2 * top, tokens), f32)
 
     def over(left, right):
         return lax.dot_general(left, right, (((0,), (0,)), ((), ())), preferred_element_type=f32)
@@ -105,12 +85,6 @@
     def against(left, right):
         return lax.dot_general(left, right, (((1,), (1,)), ((), ())), preferred_element_type=f32)
 
-    send[:, 0] = over(pick_all, mixed_ref[...]).astype(half).reshape(n, slots, width)
-    chosen = jnp.zeros((n * slots, width), f32)
-    for j in range(top):
-        scaled = upright(wts_ref[j : j + 1, :]) * cot_ref[...].astype(f32)
-        chosen = chosen + over(picks[j], scaled.astype(half))
-    send[:, 1] = chosen.astype(half).reshape(n, slots, width)
     sent = []
 
     def remote(src, dst, recv, where):
@@ -123,16 +97,90 @@
         copy.start()
         sent.append(copy)
 
-    def over_sp(k):
-        return remote(send.at[k], xbuf.at[q, k], sp_sem.at[k], {"sp": lax.rem(me + k, n)})
+    lines, held = n // 2, tok.shape[0]
+    following_line = lax.rem(me + 2, n)
+
+    def ring_copy(j, i):
+        source = (mixed_ref, cot_ref)[i] if j == 0 else tok.at[j % held, i]
+        return pltpu.make_async_remote_copy(
+            src_ref=source, dst_ref=tok.at[(j + 1) % held, i], send_sem=tok_send.at[j, i],
+            recv_sem=tok_sem.at[j + 1, i], device_id={"sp": following_line}, device_id_type=MESH,
+        )
+
+    def ring_start(j):
+        if j + 1 > held:
+            pl.semaphore_wait(credit, 1)
+        for i in range(2):
+            ring_copy(j, i).start()
+
+    def ring_free(j):
+        for i in range(2):
+            ring_copy(j, i).wait_send()
+        if 1 <= j and j + held < lines:
+            pl.semaphore_signal(
+                credit, inc=1, device_id={"sp": lax.rem(me + n - 2, n)}, device_id_type=MESH
+            )
+
+    def info_copy(j):
+        return remote(info.at[0], info.at[j], info_sem.at[j], {"sp": lax.rem(me + 2 * j, n)})
+
+    def cross_copy(j):
+        return remote(send.at[j], xbuf.at[q, 2 * j + 1], x_sem.at[j], {"sp": me ^ 1})
+
+    slot = lax.broadcasted_iota(jnp.int32, (slots, tokens), 0)
+    before = lax.broadcasted_iota(jnp.int32, (tokens, tokens), 0) < (
+        lax.broadcasted_iota(jnp.int32, (tokens, tokens), 1)
+    )
+
+    def arrive(j):
+        if j > 0:
+            for i in range(2):
+                ring_copy(j - 1, i).wait_recv()
+            if j < lines - 1:
+                ring_start(j)
+            ring_free(j - 1)
+            info_copy(j).wait_recv()
+        rows = mixed_ref[...] if j == 0 else tok[j % held, 0]
+        cots = cot_ref[...] if j == 0 else tok[j % held, 1]
+        ids = [info[j, i : i + 1, :].astype(jnp.int32) for i in range(top)]
+        which = lax.broadcasted_iota(jnp.int32, (8, tokens), 0)
+        wanted = jnp.where(which == 0, me, me ^ 1)
+        hit = jnp.zeros((8, tokens), f32)
+        weight = jnp.zeros((8, tokens), f32)
+        for i in range(top):
+            same = ids[i] == wanted
+            hit = jnp.where(same, 1.0, hit)
+            weight = jnp.where(same, info[j, top + i : top + i + 1, :], weight)
+        order = jnp.dot(
+            hit.astype(half), jnp.where(before, 1.0, 0.0).astype(half), preferred_element_type=f32
+        )
+        order = jnp.where(hit > 0.5, order, -1.0).astype(jnp.int32)
+        for side in (1, 0):
+            chosen = slot == order[side : side + 1, :]
+            pick = jnp.where(chosen, 1.0, 0.0).astype(half)
+            scale = jnp.sum(
+                jnp.where(chosen, weight[side : side + 1, :], 0.0), axis=1, keepdims=True
+            )
+            x = jnp.dot(pick, rows, preferred_element_type=f32).astype(half)
+            c = (scale * jnp.dot(pick, cots, preferred_element_type=f32)).astype(half)
+            if side == 1:
+                send[j, 0] = x
+                send[j, 1] = c
+                start(cross_copy(j))
+            else:
+                xbuf[q, 2 * j, 0] = x
+                xbuf[q, 2 * j, 1] = c
+                spread(2 * j)
+
+    def crossed(j):
+        cross_copy(j).wait_recv()
+        spread(2 * j + 1)
 
     def over_tp(owner, k, other, sems):
         spot = xbuf.at[owner, k]
         return remote(spot, spot, sems.at[k], {"tp": other})
 
     def spread(k):
-        if k > 0:
-            over_sp(k).wait_recv()
         start(over_tp(q, k, far, y_sem))
         start(over_tp(q, k, near, own_sem))
 
@@ -185,7 +233,8 @@
     def back_copy(g, i):
         k = g * per + i
         return remote(
-            rbuf.at[g, i], ret.at[k], ret_sem.at[k], {"sp": lax.rem(me + n - k, n)}
+            rbuf.at[g, i], ret.at[k], ret_sem.at[k],
+            {"sp": lax.rem(me + n - 2 * (k // 2), n) ^ (k % 2)},
         )
 
     def join_far(g):
@@ -215,8 +264,6 @@
             acc_u[cols, :] += both[:, hidden:]
             acc_d[:, cols] += down
 
-    lines = n // 2
-
     def ring_source(j):
         return lax.rem(me + n - 2 * j, n)
 
@@ -233,10 +280,10 @@
         ring_send(j, source)
 
     pl.semaphore_wait(barrier, n + 1)
-    for k in range(1, n):
-        start(over_sp(k))
-    xbuf[q, 0] = send[0]
-    spread(0)
+    ring_start(0)
+    for j in range(1, lines):
+        start(info_copy(j))
+    arrive(0)
 
     total = width
     row = lax.broadcasted_iota(jnp.int32, (8, total), 0)
@@ -300,37 +347,42 @@
             prods[at, :] = p
             carry_p = p[0:1, :]
 
-    fillers = [forward, forward_scan, forward_gate, back_products]
-    for fill in fillers[:3]:
-        fill()
-    late = [fillers[3]]
+    forward()
+    forward_scan()
+    crossed(0)
+    relay(0)
+    forward_gate()
+    back_products()
     for copy in loads:
         copy.wait()
     grad_chunks = [functools.partial(grads, 0, b) for b in range(parts)]
     steps = [functools.partial(ring, j) for j in range(lines)]
-    for k in range(1, n + 1):
-        if k < n:
-            spread(k)
-        relay(k - 1)
-        if k == 1:
-            back_products()
-        if k >= per + 1 and (k - 1) % per == 0:
-            g = (k - 1) // per - 1
-            expert(g)
-            if g >= 1:
-                join_near(g - 1)
+    line_group = per // 2
+    for j in range(1, lines):
+        arrive(j)
+        relay(2 * j - 1)
+        if j == lines - 1:
+            steps.pop(0)()
+        g = j // line_group
+        if j % line_group == 0:
+            expert(g - 1)
             if g >= 2:
-                join_far(g - 2)
-        if k > 2 * per + 1 and (k - 1) % per != 0 and grad_chunks:
+                join_near(g - 2)
+            if g >= 3:
+                join_far(g - 3)
+        crossed(j)
+        relay(2 * j)
+        if g > groups // 2 and grad_chunks:
             grad_chunks.pop(0)()
-        if k == n - 1:
-            steps.pop(0)()
     last = groups - 1
+    join_near(last - 1)
+    relay(n - 1)
+    steps.pop(0)()
     expert(last)
-    join_near(last - 1)
-    steps.pop(0)()
     join_far(last - 2)
     join_near(last)
+    if steps:
+        steps.pop(0)()
     while grad_chunks:
         grad_chunks.pop(0)()
     join_far(last - 1)
@@ -345,6 +397,28 @@
         copy = pltpu.make_async_copy(src, dst, g_sem.at[i])
         copy.start()
         g_copies.append(copy)
+    lane = lax.broadcasted_iota(jnp.int32, (tokens, 128), 1)
+    away = []
+    for j in range(top):
+        named = upright(info[0, j : j + 1, :]).astype(jnp.int32)
+        gap = lax.shift_right_logical(named, 1) - lax.div(me, 2)
+        gap = jnp.where(gap < 0, gap + lines, gap)
+        away.append(2 * gap + ((named ^ me) & 1))
+    member = jnp.zeros((tokens, 128), f32)
+    for j in range(top):
+        member = jnp.where(away[j] == lane, 1.0, member)
+    earlier = lax.broadcasted_iota(jnp.int32, (tokens, tokens), 1) < (
+        lax.broadcasted_iota(jnp.int32, (tokens, tokens), 0)
+    )
+    rank = jnp.dot(
+        jnp.where(earlier, 1.0, 0.0).astype(half), member.astype(half), preferred_element_type=f32
+    )
+    place = lax.broadcasted_iota(jnp.int32, (tokens, n * slots), 1)
+    pick_all = jnp.zeros((tokens, n * slots), f32)
+    for j in range(top):
+        mine = jnp.sum(jnp.where(away[j] == lane, rank, 0.0), axis=1, keepdims=True)
+        pick_all = jnp.where(place == away[j] * slots + mine.astype(jnp.int32), 1.0, pick_all)
+    pick_all = pick_all.astype(half)
     for k in range(1, n):
         back_copy(k // per, k % per).wait_recv()
     summed = jnp.dot(pick_all, ret[...].reshape(n * slots, width), preferred_element_type=f32)
@@ -502,7 +576,9 @@
         scratch_shapes=[
             vm((full, hidden), half), vm((full, hidden), half), vm((hidden, full), half),
             vm((width, full), half),
-            vm((n, 2, slots, width), half),
+            vm((n // 2, 8, tokens), f32),
+            vm((min(n // 2, 8), 2, tokens, width), half),
+            vm((n // 2, 2, slots, width), half),
             vm((parts, n, 2, slots, width), half),
             vm((n * slots, 2 * hidden), half), vm((n * slots, hidden), half),
             vm((groups, parts, block, width), half),
@@ -520,7 +596,8 @@
             vm((some, tokens, thin), half),
             vm((8, width), f32),
             vm((n, 8, width), f32),
-            dma((2,)), dma((n,)), dma((n,)), dma((n,)), dma((n,)), dma((groups, 2)),
+            dma((2,)), dma((n // 2, 2)), pltpu.SemaphoreType.REGULAR, dma((n // 2, 2)), dma((n // 2,)), dma((n // 2,)), dma((n,)), dma((n,)), dma((n,)),
+            dma((groups, 2)),
             dma((groups,)), dma((n,)), dma((3,)), dma((4,)), dma((3,)),
             dma((n // 2,)), dma((n // 2,)), dma((n,)), dma((3,)), dma((n,)),
         ],

time: 128 us -> 115 us (0.90)
  the two profiles are of different devices: /device:TPU:0 before, /device:TPU:3 now
where the time goes in v3:
time: 115 us; the launch traced here: 114 us
  Pallas kernels  105 us (91%)
  local copies, waits for them, and re-layouts  9.07 us (8%)
    pallas_call x1, Pallas kernels, run_whole(): pl.pallas_call(functools.partial(whole_kernel, n, groups), out_shape=(sha...  105 us
    unnamed x16, local copies, waits for them, and re-layouts  9.07 us

profile of v3, /device:TPU:3, one launch (start us, length us, event | category | flops | bytes accessed | tf_op | source)
XLA Modules:
  0.0 114.5 jit_solution(4119377871555904617)
XLA Ops:
  0.6 104.7 %shard_map.190 = (f32[2048,256]{1,0:T(8,128)}, f32[2048,256]{1,0:T(8,128)}, f32[256,2048]{1,0:T(8,128)}, f32[256,512]{1,0:T(8,128)}, bf16[192,512]{1,0:T(8,128)(2,1)}, /*index=5*/bf16[192,512]{1,0:T(8,128)(2,1)}) custom-call(bf16[192,512]{1,0:T(8,128)(2,1)} %mixed_ref.1, bf16[192,512]{1,0:T(8,128)(2,1)} %cot_ref.1, s32[2,192]{1,0:T(2,128)} %bitcast.16, ...), custom_call_target="tpu_custom_call" | custom-call | flops 8000000000 | bytes 80000000 | tf_op jit(solution)/shard_map/pallas_call | solution.py:568
  105.4 0.0 copy-start.1
  105.4 3.2 %copy.27 = f32[1,2048,256]{2,1,0:T(8,128)} copy(f32[1,2048,256]{2,1,0:T(8,128)} %bitcast.12) | data formatting | bytes 4194304
  108.6 0.0 copy-done.1
  108.6 0.0 copy-start
  108.6 1.3 %copy.28 = f32[1,2048,256]{2,1,0:T(8,128)} copy(f32[1,2048,256]{2,1,0:T(8,128)S(1)} %bitcast.11) | data formatting | bytes 4194304
  109.9 1.0 copy-done
  110.9 0.0 copy-start.2
  110.9 0.0 copy-start.4
  110.9 0.0 copy-start.3
  110.9 1.3 %copy.29 = f32[1,256,2048]{2,1,0:T(8,128)} copy(f32[1,256,2048]{2,1,0:T(8,128)S(1)} %bitcast.10) | data formatting | bytes 4194304
  112.2 0.0 copy-done.2
  112.3 0.8 copy.30
  113.1 0.0 copy-done.4
  113.1 0.7 copy.31
  113.8 0.0 copy-done.3
  113.8 0.7 copy.32
Async XLA Ops:
  105.4 3.2 %copy-start.1 = (f32[2048,256]{1,0:T(8,128)S(1)}, f32[2048,256]{1,0:T(8,128)}, u32[]{:S(2)}) copy-start(f32[2048,256]{1,0:T(8,128)} %get-tuple-element.13) | copy-start | bytes 6291460
  108.6 2.3 %copy-start = (f32[256,2048]{1,0:T(8,128)S(1)}, f32[256,2048]{1,0:T(8,128)}, u32[]{:S(2)}) copy-start(f32[256,2048]{1,0:T(8,128)} %get-tuple-element.14) | copy-start | bytes 6291460
  110.9 1.4 %copy-start.2 = (f32[256,512]{1,0:T(8,128)S(1)}, f32[256,512]{1,0:T(8,128)}, u32[]{:S(2)}) copy-start(f32[256,512]{1,0:T(8,128)} %get-tuple-element.27) | copy-start | bytes 1572868
  110.9 2.2 %copy-start.4 = (bf16[192,512]{1,0:T(8,128)(2,1)S(1)}, bf16[192,512]{1,0:T(8,128)(2,1)}, u32[]{:S(2)}) copy-start(bf16[192,512]{1,0:T(8,128)(2,1)} %get-tuple-element.28) | copy-start | bytes 589828
  110.9 2.8 %copy-start.3 = (bf16[192,512]{1,0:T(8,128)(2,1)S(1)}, bf16[192,512]{1,0:T(8,128)(2,1)}, u32[]{:S(2)}) copy-start(bf16[192,512]{1,0:T(8,128)(2,1)} %get-tuple-element.29) | copy-start | bytes 589828

commit v4 on v3

--- a/solution.py
+++ b/solution.py
@@ -32,14 +32,16 @@
 
 def whole_kernel(
     n, groups,
+    mixed_hbm, cot_hbm, ids_hbm, wts_hbm,
+    conv_hbm, gate_hbm, bs_hbm, param_hbm, shift_hbm, wr_hbm, wi_hbm,
+    wg_hbm, wu_hbm, wd_hbm, wo_hbm,
+    acc_g, acc_u, acc_d, go_ref, out_ref, gate_out_ref,
     mixed_ref, cot_ref, ids_ref, wts_ref,
     conv_ref, gate_ref, bs_ref, param_ref, shift_ref, wr_ref, wi_ref,
-    wg_hbm, wu_hbm, wd_hbm, wo_hbm,
-    gg_hbm, gu_hbm, gd_hbm, go_ref, out_ref, gate_out_ref,
     wg, wu, wd, wo, info, tok, send, xbuf, dbuf, hbuf, pbuf, nbuf, sbuf, fbuf, rbuf, ret, dcols, dmbuf,
-    acc_g, acc_u, acc_d, dec, drive, st, act_b, slope_b, fac_r, fac_i, fac_o, prods, lev0, lev1, lev2, grad,
+    dec, drive, st, act_b, slope_b, fac_r, fac_i, fac_o, prods, lev0, lev1, lev2, grad,
     mg, got, bsend, mine_pair, pairs,
-    send_sem, tok_send, credit, tok_sem, info_sem, x_sem, y_sem, own_sem, fwd_sem, near_sem, far_sem, ret_sem, dm_sem, w_sem, g_sem,
+    send_sem, tok_send, credit, tok_sem, info_sem, x_sem, y_sem, own_sem, fwd_sem, near_sem, far_sem, ret_sem, dm_sem, w_sem,
     mz_sem, mx_sem, blk_sem, got_sem, pair_sem,
 ):
     me, q = lax.axis_index("sp"), lax.axis_index("tp")
@@ -51,9 +53,14 @@
         )
     for other in (near, far):
         pl.semaphore_signal(barrier, inc=1, device_id={"tp": other}, device_id_type=MESH)
+    pairs_in = (
+        (ids_hbm, ids_ref), (wts_hbm, wts_ref), (mixed_hbm, mixed_ref), (cot_hbm, cot_ref),
+        (conv_hbm, conv_ref), (gate_hbm, gate_ref), (bs_hbm, bs_ref), (param_hbm, param_ref),
+        (shift_hbm, shift_ref), (wr_hbm, wr_ref), (wi_hbm, wi_ref),
+        (wg_hbm, wg), (wu_hbm, wu), (wd_hbm, wd), (wo_hbm, wo),
+    )
     loads = [
-        pltpu.make_async_copy(src, dst, w_sem.at[i])
-        for i, (src, dst) in enumerate(((wg_hbm, wg), (wu_hbm, wu), (wd_hbm, wd), (wo_hbm, wo)))
+        pltpu.make_async_copy(src, dst, w_sem.at[i]) for i, (src, dst) in enumerate(pairs_in)
     ]
     for copy in loads:
         copy.start()
@@ -74,6 +81,8 @@
     def upright(row):
         return jnp.sum(jnp.where(eye, row, jnp.zeros_like(row)), axis=1, keepdims=True)
 
+    for copy in loads[:2]:
+        copy.wait()
     for j in range(top):
         info[0, j : j + 1, :] = ids_ref[j : j + 1, :].astype(f32)
         info[0, top + j : top + j + 1, :] = wts_ref[j : j + 1, :]
@@ -101,7 +110,7 @@
     following_line = lax.rem(me + 2, n)
 
     def ring_copy(j, i):
-        source = (mixed_ref, cot_ref)[i] if j == 0 else tok.at[j % held, i]
+        source = (mixed_hbm, cot_hbm)[i] if j == 0 else tok.at[j % held, i]
         return pltpu.make_async_remote_copy(
             src_ref=source, dst_ref=tok.at[(j + 1) % held, i], send_sem=tok_send.at[j, i],
             recv_sem=tok_sem.at[j + 1, i], device_id={"sp": following_line}, device_id_type=MESH,
@@ -138,7 +147,6 @@
                 ring_copy(j - 1, i).wait_recv()
             if j < lines - 1:
                 ring_start(j)
-            ring_free(j - 1)
             info_copy(j).wait_recv()
         rows = mixed_ref[...] if j == 0 else tok[j % held, 0]
         cots = cot_ref[...] if j == 0 else tok[j % held, 1]
@@ -171,6 +179,8 @@
                 xbuf[q, 2 * j, 0] = x
                 xbuf[q, 2 * j, 1] = c
                 spread(2 * j)
+        if j > 0:
+            ring_free(j - 1)
 
     def crossed(j):
         cross_copy(j).wait_recv()
@@ -283,6 +293,8 @@
     ring_start(0)
     for j in range(1, lines):
         start(info_copy(j))
+    for copy in loads[2:4]:
+        copy.wait()
     arrive(0)
 
     total = width
@@ -347,13 +359,15 @@
             prods[at, :] = p
             carry_p = p[0:1, :]
 
+    for copy in loads[4:11]:
+        copy.wait()
     forward()
     forward_scan()
     crossed(0)
     relay(0)
     forward_gate()
     back_products()
-    for copy in loads:
+    for copy in loads[11:]:
         copy.wait()
     grad_chunks = [functools.partial(grads, 0, b) for b in range(parts)]
     steps = [functools.partial(ring, j) for j in range(lines)]
@@ -361,7 +375,7 @@
     for j in range(1, lines):
         arrive(j)
         relay(2 * j - 1)
-        if j == lines - 1:
+        if j == max(1, lines - 2):
             steps.pop(0)()
         g = j // line_group
         if j % line_group == 0:
@@ -376,8 +390,10 @@
             grad_chunks.pop(0)()
     last = groups - 1
     join_near(last - 1)
+    steps.pop(0)()
     relay(n - 1)
-    steps.pop(0)()
+    if steps:
+        steps.pop(0)()
     expert(last)
     join_far(last - 2)
     join_near(last)
@@ -392,11 +408,6 @@
     join_far(last)
     for b in range(1, parts):
         grads(1, b)
-    g_copies = []
-    for i, (src, dst) in enumerate(((acc_g, gg_hbm), (acc_u, gu_hbm), (acc_d, gd_hbm))):
-        copy = pltpu.make_async_copy(src, dst, g_sem.at[i])
-        copy.start()
-        g_copies.append(copy)
     lane = lax.broadcasted_iota(jnp.int32, (tokens, 128), 1)
     away = []
     for j in range(top):
@@ -476,21 +487,6 @@
         other = q ^ shift_by
         at = pl.ds(pl.multiple_of(other * width, width), width)
         grad[...] += against(dmbuf[other], wo[:, at])
-    for off in range(1, n):
-        blk_wait(lax.rem(me + off, n))
-
-    @pl.when(q != owner_q)
-    def _():
-        blk_wait(me)
-
-    def got_copy(part, i, other):
-        at = pl.ds(pl.multiple_of(part * quarter, quarter), quarter)
-        spot = got.at[:, at]
-        return remote(spot, spot, got_sem.at[i], {"tp": other})
-
-    start(got_copy(q, 0, far))
-    start(got_copy(q, 1, near))
-
     carry = jnp.zeros((1, total), f32)
     for i in reversed(range(tokens // 8)):
         at = slice(8 * i, 8 * i + 8)
@@ -514,8 +510,21 @@
 
     for off in range(1, n):
         start(pair_to(lax.rem(me + off, n), me))
-    got_copy(far, 0, far).wait_recv()
-    start(got_copy(far, 2, near))
+    for off in range(1, n):
+        blk_wait(lax.rem(me + off, n))
+
+    @pl.when(q != owner_q)
+    def _():
+        blk_wait(me)
+
+    def got_copy(part, i, other):
+        at = pl.ds(pl.multiple_of(part * quarter, quarter), quarter)
+        spot = got.at[:, at]
+        return remote(spot, spot, got_sem.at[i], {"tp": other})
+
+    start(got_copy(q, 0, far))
+    start(got_copy(q, 1, near))
+
     for off in range(1, n):
         peer = lax.rem(me + off, n)
         pair_to(peer, peer).wait_recv()
@@ -531,14 +540,14 @@
         out_ref[:, cols] = (
             g * fac_o[:, cols] + against(d_r, wr_ref[h]) + against(d_i, wi_ref[h])
         ).astype(half)
+    got_copy(far, 0, far).wait_recv()
+    start(got_copy(far, 2, near))
     for j in range(lines):
         spot = mg.at[ring_source(j) ^ 1]
         remote(spot, spot, mx_sem.at[j], {"sp": me ^ 1}).wait_recv()
     got_copy(near, 1, near).wait_recv()
     got_copy(near ^ 2, 2, near).wait_recv()
     go_ref[...] = over(got[...].reshape(n * tokens, thin), mg[...].reshape(n * tokens, width))
-    for copy in g_copies:
-        copy.wait()
     for copy in sent:
         copy.wait_send()
     for i in range(some):
@@ -564,16 +573,16 @@
     half, f32 = jnp.bfloat16, jnp.float32
     anywhere = pl.BlockSpec(memory_space=pl.ANY)
     dma, vm = pltpu.SemaphoreType.DMA, pltpu.VMEM
-    shape = jax.ShapeDtypeStruct
+    small = (mixed, cot, ids, weights, conv, gate, bs, param, shift, wr, wi)
     return pl.pallas_call(
         functools.partial(whole_kernel, n, groups),
         out_shape=(
-            shape((full, hidden), f32), shape((full, hidden), f32), shape((hidden, full), f32),
-            shape((thin, width), f32), shape((tokens, width), half), shape((tokens, width), half),
+            vm((full, hidden), f32), vm((full, hidden), f32), vm((hidden, full), f32),
+            vm((thin, width), f32), vm((tokens, width), half), vm((tokens, width), half),
         ),
-        in_specs=[VM] * 11 + [anywhere] * 4,
-        out_specs=(anywhere,) * 3 + (VM,) * 3,
-        scratch_shapes=[
+        in_specs=[anywhere] * 15,
+        out_specs=(VM,) * 6,
+        scratch_shapes=[vm(a.shape, a.dtype) for a in small] + [
             vm((full, hidden), half), vm((full, hidden), half), vm((hidden, full), half),
             vm((width, full), half),
             vm((n // 2, 8, tokens), f32),
@@ -589,7 +598,6 @@
             vm((n, slots, width), half),
             vm((tokens, width), half),
             vm((parts, tokens, width), half),
-            vm((full, hidden), f32), vm((full, hidden), f32), vm((hidden, full), f32),
         ] + [vm((tokens, width), f32)] * 13 + [
             vm((n, tokens, width), half),
             vm((n, tokens, thin), half),
@@ -598,14 +606,37 @@
             vm((n, 8, width), f32),
             dma((2,)), dma((n // 2, 2)), pltpu.SemaphoreType.REGULAR, dma((n // 2, 2)), dma((n // 2,)), dma((n // 2,)), dma((n,)), dma((n,)), dma((n,)),
             dma((groups, 2)),
-            dma((groups,)), dma((n,)), dma((3,)), dma((4,)), dma((3,)),
+            dma((groups,)), dma((n,)), dma((3,)), dma((15,)),
             dma((n // 2,)), dma((n // 2,)), dma((n,)), dma((3,)), dma((n,)),
         ],
         compiler_params=pltpu.CompilerParams(
-            collective_id=0, has_side_effects=True, vmem_limit_bytes=63000 * 1024
+            collective_id=0, has_side_effects=True, vmem_limit_bytes=55000 * 1024
         ),
         cost_estimate=pl.CostEstimate(flops=8_000_000_000, bytes_accessed=80_000_000, transcendentals=0),
     )(mixed, cot, ids, weights, conv, gate, bs, param, shift, wr, wi, wg, wu, wd, wo)
+
+
+def write_kernel(*refs):
+    count = len(refs) // 2
+    copies = [
+        pltpu.make_async_copy(refs[i], refs[count + i], refs[-1].at[i]) for i in range(count)
+    ]
+    for copy in copies:
+        copy.start()
+    for copy in copies:
+        copy.wait()
+
+
+def write_out(*arrays):
+    held = [pltpu.with_memory_space_constraint(a, pltpu.VMEM) for a in arrays]
+    return pl.pallas_call(
+        write_kernel,
+        out_shape=tuple(jax.ShapeDtypeStruct(a.shape, a.dtype) for a in arrays),
+        in_specs=[VM] * len(arrays),
+        out_specs=(pl.BlockSpec(memory_space=pl.ANY),) * len(arrays),
+        scratch_shapes=[pltpu.SemaphoreType.DMA((len(arrays),))],
+        compiler_params=pltpu.CompilerParams(vmem_limit_bytes=1024 * 1024),
+    )(*held)
 
 
 def body(
@@ -616,11 +647,12 @@
     experts = lax.axis_size("sp")
     capacity = 2 * tok_rows * top_k // experts
     slots = -(-capacity // 16) * 16
-    grad_gate_e, grad_up_e, grad_down_e, grad_out, grad_in, grad_gate = run_whole(
+    results = run_whole(
         experts, lax.axis_size("tp"), slots, mixed, d_out, expert_ids.T, route_weights.T,
         conv_out, gate_in, block_states, decay_param[None, :], decay_shift[None, :],
         w_reset, w_input, w_gate[0], w_up[0], w_down[0], w_out,
     )
+    grad_gate_e, grad_up_e, grad_down_e, grad_out, grad_in, grad_gate = write_out(*results)
     return (grad_gate_e[None], grad_up_e[None], grad_down_e[None], grad_out, grad_in, grad_gate)
 
 

time: 115 us -> 101 us (0.88)
  the two profiles are of different devices: /device:TPU:3 before, /device:TPU:0 now
where the time goes in v4:
time: 101 us
  Pallas kernels  100 us (99%)
    pallas_call x1, Pallas kernels, run_whole(): pl.pallas_call(functools.partial(whole_kernel, n, groups), out_shape=(vm(...  97 us
    pallas_call x1, Pallas kernels, write_out(): pl.pallas_call(write_kernel, out_shape=tuple((jax.ShapeDtypeStruct(a.shap...  2.96 us

profile of v4, /device:TPU:0, one launch (start us, length us, event | category | flops | bytes accessed | tf_op | source)
XLA Modules:
  0.0 100.6 jit_solution(1847269822121425156)
XLA Ops:
  0.6 97.0 %shard_map.190 = (f32[2048,256]{1,0:T(8,128)S(1)}, f32[2048,256]{1,0:T(8,128)S(1)}, f32[256,2048]{1,0:T(8,128)S(1)}, f32[256,512]{1,0:T(8,128)S(1)}, bf16[192,51...) custom-call(bf16[192,512]{1,0:T(8,128)(2,1)} %mixed_hbm.1, bf16[192,512]{1,0:T(8,128)(2,1)} %cot_hbm.1, ...), custom_call_target="tpu_custom_call" | custom-call | flops 8000000000 | bytes 80000000 | tf_op jit(solution)/shard_map/pallas_call | solution.py:577
  97.7 3.0 %shard_map.191 = (f32[2048,256]{1,0:T(8,128)}, f32[2048,256]{1,0:T(8,128)}, f32[256,2048]{1,0:T(8,128)}, f32[256,512]{1,0:T(8,128)}, bf16[192,512]{1,0:T(8,128)(2,1)}, /*index=5*/bf16[192,512]{1,0:T(8,128)(2,1)}) custom-call(f32[2048,256]{1,0:T(8,128)S(1)} %get-tuple-element.18.refs_0_, f32[2048,256]{1,0:T(8,128)S(1)} %get-tuple-element.19.refs_1_, ...), custom_call_target="tpu_custom_call" | custom-call | tf_op jit(solution)/shard_map/pallas_call | solution.py:632

commit v5 on v4

--- a/solution.py
+++ b/solution.py
@@ -40,7 +40,7 @@
     conv_ref, gate_ref, bs_ref, param_ref, shift_ref, wr_ref, wi_ref,
     wg, wu, wd, wo, info, tok, send, xbuf, dbuf, hbuf, pbuf, nbuf, sbuf, fbuf, rbuf, ret, dcols, dmbuf,
     dec, drive, st, act_b, slope_b, fac_r, fac_i, fac_o, prods, lev0, lev1, lev2, grad,
-    mg, got, bsend, mine_pair, pairs,
+    mg, got, bsend, bfar, mine_pair, pairs,
     send_sem, tok_send, credit, tok_sem, info_sem, x_sem, y_sem, own_sem, fwd_sem, near_sem, far_sem, ret_sem, dm_sem, w_sem,
     mz_sem, mx_sem, blk_sem, got_sem, pair_sem,
 ):
@@ -369,45 +369,40 @@
     back_products()
     for copy in loads[11:]:
         copy.wait()
-    grad_chunks = [functools.partial(grads, 0, b) for b in range(parts)]
+    grad_chunks = [functools.partial(grads, h, b) for h in range(2) for b in range(parts)]
     steps = [functools.partial(ring, j) for j in range(lines)]
+
+    def some_of(work, count):
+        for _ in range(min(count, len(work))):
+            work.pop(0)()
+
     line_group = per // 2
     for j in range(1, lines):
+        g = j // line_group if j % line_group == 0 else 0
         arrive(j)
+        if g == 3:
+            join_far(1)
         relay(2 * j - 1)
-        if j == max(1, lines - 2):
-            steps.pop(0)()
-        g = j // line_group
-        if j % line_group == 0:
+        if j == max(1, lines - 2) or g == 3:
+            some_of(steps, 1)
+        if g:
             expert(g - 1)
-            if g >= 2:
-                join_near(g - 2)
-            if g >= 3:
-                join_far(g - 3)
+        if g == 2:
+            join_near(1)
         crossed(j)
         relay(2 * j)
-        if g > groups // 2 and grad_chunks:
-            grad_chunks.pop(0)()
-    last = groups - 1
-    join_near(last - 1)
-    steps.pop(0)()
+    join_near(2)
     relay(n - 1)
-    if steps:
-        steps.pop(0)()
-    expert(last)
-    join_far(last - 2)
-    join_near(last)
-    if steps:
-        steps.pop(0)()
-    while grad_chunks:
-        grad_chunks.pop(0)()
-    join_far(last - 1)
-    grads(1, 0)
-    if steps:
-        steps.pop(0)()
-    join_far(last)
-    for b in range(1, parts):
-        grads(1, b)
+    some_of(steps, 1)
+    expert(3)
+    join_near(3)
+    join_near(0)
+    join_far(2)
+    some_of(grad_chunks, 4)
+    some_of(steps, 1)
+    join_far(3)
+    some_of(grad_chunks, 4)
+    join_far(0)
     lane = lax.broadcasted_iota(jnp.int32, (tokens, 128), 1)
     away = []
     for j in range(top):
@@ -437,22 +432,92 @@
 
     some = n // parts
     thin = width // some
-    quarter = tokens // parts
-    owner_q = lax.div(me, some)
-
-    def blk_copy(i, x):
-        peer, part = q * some + i, q ^ x
-        at = pl.ds(pl.multiple_of(part * quarter, quarter), quarter)
+    big, little = tokens // 3, tokens // 6
+    owner = lax.div(me, some)
+    apart = q ^ owner
+    place_in = apart & 1
+
+    def blk_copy(source, i, peer, other, first, size):
         return pltpu.make_async_remote_copy(
-            src_ref=bsend.at[i, at], dst_ref=got.at[me, at], send_sem=send_sem.at[1],
-            recv_sem=blk_sem.at[me], device_id={"sp": peer, "tp": part}, device_id_type=MESH,
+            src_ref=source.at[i, first : first + size],
+            dst_ref=got.at[me, pl.ds(first, size)],
+            send_sem=send_sem.at[1], recv_sem=blk_sem.at[me],
+            device_id={"sp": peer, "tp": other}, device_id_type=MESH,
         )
 
-    mine_at = pl.ds(pl.multiple_of(q * quarter, quarter), quarter)
-
-    def blk_wait(source):
-        spot = got.at[source, mine_at]
-        remote(spot, spot, blk_sem.at[source], {"tp": far}).wait_recv()
+    blocks_sent = []
+
+    def blk_send(source, held, first, size):
+        for i in range(some):
+            peer = held * some + i
+            start(blk_copy(source, i, peer, near, first + size, size))
+            mine = blk_copy(source, i, peer, q, first, size)
+            blocks_sent.append((peer, mine))
+
+            @pl.when(peer != me)
+            def _():
+                mine.start()
+
+            @pl.when(peer == me)
+            def _():
+                got[me, first : first + size] = source[i, first : first + size]
+
+    def rows_big(part):
+        return pl.ds(pl.multiple_of(part * big, big), big)
+
+    def rows_little(part):
+        return pl.ds(pl.multiple_of(2 * big + part * little, little), little)
+
+    def rows_of(mine, part, inside):
+        return rows_big(part) if mine == inside else rows_little(part)
+
+    def got_copy(inside, mine, part, i, other):
+        spot = got.at[:, rows_of(mine, part, inside)]
+        return pltpu.make_async_remote_copy(
+            src_ref=spot, dst_ref=spot, send_sem=send_sem.at[1], recv_sem=got_sem.at[i],
+            device_id={"tp": other}, device_id_type=MESH,
+        )
+
+    def share(inside):
+        spot_rows = rows_of(True, place_in, inside)
+        for off in range(1, n):
+            source = lax.rem(me + off, n)
+            spot = got.at[source, spot_rows]
+            remote(spot, spot, blk_sem.at[source], {"tp": far}).wait_recv()
+
+        @pl.when(place_in == 1)
+        def _():
+            spot = got.at[me, spot_rows]
+            remote(spot, spot, blk_sem.at[me], {"tp": far}).wait_recv()
+
+        got_copy(inside, True, place_in, 0, far).start()
+        got_copy(inside, True, place_in, 1, near).start()
+
+    def share_on(inside):
+        got_copy(inside, False, place_in, 0, far).wait_recv()
+        got_copy(inside, False, place_in, 2, near).start()
+
+    def project(inside, mine, part):
+        at = rows_of(mine, part, inside)
+        count = n * (big if mine == inside else little)
+        return over(got[:, at, :].reshape(count, thin), mg[:, at, :].reshape(count, width))
+
+    def project_own(inside):
+        go_ref[...] = project(inside, True, place_in)
+
+    def project_rest(inside):
+        go_ref[...] += project(inside, False, place_in)
+        got_copy(inside, True, place_in ^ 1, 1, near).wait_recv()
+        go_ref[...] += project(inside, True, place_in ^ 1)
+        got_copy(inside, False, place_in ^ 1, 2, near).wait_recv()
+        go_ref[...] += project(inside, False, place_in ^ 1)
+        for i, other in ((0, far), (1, near)):
+            got_copy(inside, True, place_in, i, other).wait_send()
+        got_copy(inside, False, place_in, 2, near).wait_send()
+
+    def each(work, *sides):
+        for inside in sides:
+            pl.when((apart < 2) == inside)(functools.partial(work, inside))
 
     def dm_copy(owner, i, other, src):
         return remote(src, dmbuf.at[owner], dm_sem.at[i], {"tp": other})
@@ -461,18 +526,7 @@
     start(dm_copy(q, 1, near, dcols))
     for i in range(some):
         bsend[i] = dcols[:, i * thin : (i + 1) * thin]
-    for i in range(some):
-        for x in range(1, parts):
-            start(blk_copy(i, x))
-
-        @pl.when(q * some + i != me)
-        def _():
-            blk_copy(i, 0).start()
-
-        @pl.when(q * some + i == me)
-        def _():
-            got[me, mine_at] = bsend[i, mine_at]
-
+    blk_send(bsend, q, 0, big)
     while steps:
         steps.pop(0)()
     dmbuf[q] = dcols[...]
@@ -481,12 +535,16 @@
     grad[...] = against(dcols[...], wo[:, wo_cols])
     dm_copy(far, 0, far, dcols).wait_recv()
     start(dm_copy(far, 2, near, dmbuf.at[far]))
+    for i in range(some):
+        bfar[i, 2 * big :, :] = dmbuf[far, 2 * big :, i * thin : (i + 1) * thin]
+    blk_send(bfar, far, 2 * big, little)
     dm_copy(near, 1, near, dcols).wait_recv()
     dm_copy(near ^ 2, 2, near, dcols).wait_recv()
     for shift_by in (1, 2, 3):
         other = q ^ shift_by
         at = pl.ds(pl.multiple_of(other * width, width), width)
         grad[...] += against(dmbuf[other], wo[:, at])
+    each(share, True)
     carry = jnp.zeros((1, total), f32)
     for i in reversed(range(tokens // 8)):
         at = slice(8 * i, 8 * i + 8)
@@ -510,25 +568,16 @@
 
     for off in range(1, n):
         start(pair_to(lax.rem(me + off, n), me))
-    for off in range(1, n):
-        blk_wait(lax.rem(me + off, n))
-
-    @pl.when(q != owner_q)
-    def _():
-        blk_wait(me)
-
-    def got_copy(part, i, other):
-        at = pl.ds(pl.multiple_of(part * quarter, quarter), quarter)
-        spot = got.at[:, at]
-        return remote(spot, spot, got_sem.at[i], {"tp": other})
-
-    start(got_copy(q, 0, far))
-    start(got_copy(q, 1, near))
-
+    each(share, False)
+    for j in range(lines):
+        spot = mg.at[ring_source(j) ^ 1]
+        remote(spot, spot, mx_sem.at[j], {"sp": me ^ 1}).wait_recv()
+    each(project_own, True, False)
     for off in range(1, n):
         peer = lax.rem(me + off, n)
         pair_to(peer, peer).wait_recv()
     enter = jnp.zeros((1, total), f32)
+    each(share_on, True, False)
     for p in reversed(range(n)):
         pair = pairs[p]
         enter = jnp.where(p > me, pair[1:2, :] + pair[0:1, :] * enter, enter)
@@ -540,21 +589,14 @@
         out_ref[:, cols] = (
             g * fac_o[:, cols] + against(d_r, wr_ref[h]) + against(d_i, wi_ref[h])
         ).astype(half)
-    got_copy(far, 0, far).wait_recv()
-    start(got_copy(far, 2, near))
-    for j in range(lines):
-        spot = mg.at[ring_source(j) ^ 1]
-        remote(spot, spot, mx_sem.at[j], {"sp": me ^ 1}).wait_recv()
-    got_copy(near, 1, near).wait_recv()
-    got_copy(near ^ 2, 2, near).wait_recv()
-    go_ref[...] = over(got[...].reshape(n * tokens, thin), mg[...].reshape(n * tokens, width))
+    each(project_rest, True, False)
     for copy in sent:
         copy.wait_send()
-    for i in range(some):
-
-        @pl.when(q * some + i != me)
+    for peer, copy in blocks_sent:
+
+        @pl.when(peer != me)
         def _():
-            blk_copy(i, 0).wait_send()
+            copy.wait_send()
 
 
 VM = pl.BlockSpec(memory_space=pltpu.VMEM)
@@ -602,6 +644,7 @@
             vm((n, tokens, width), half),
             vm((n, tokens, thin), half),
             vm((some, tokens, thin), half),
+            vm((some, tokens, thin), half),
             vm((8, width), f32),
             vm((n, 8, width), f32),
             dma((2,)), dma((n // 2, 2)), pltpu.SemaphoreType.REGULAR, dma((n // 2, 2)), dma((n // 2,)), dma((n // 2,)), dma((n,)), dma((n,)), dma((n,)),
@@ -610,7 +653,7 @@
             dma((n // 2,)), dma((n // 2,)), dma((n,)), dma((3,)), dma((n,)),
         ],
         compiler_params=pltpu.CompilerParams(
-            collective_id=0, has_side_effects=True, vmem_limit_bytes=55000 * 1024
+            collective_id=0, has_side_effects=True, vmem_limit_bytes=57000 * 1024
         ),
         cost_estimate=pl.CostEstimate(flops=8_000_000_000, bytes_accessed=80_000_000, transcendentals=0),
     )(mixed, cot, ids, weights, conv, gate, bs, param, shift, wr, wi, wg, wu, wd, wo)

time: 101 us -> 93.7 us (0.928)
  Pallas kernels: 100 us -> 92.8 us
    pallas_call x1, Pallas kernels: 97 us -> 89.8 us  [run_whole(): pl.pallas_call(functools.partial(whole_kernel, n, groups), out_shape=(vm(...]
where the time goes in v5:
time: 93.7 us; the launch traced here: 93.4 us
  Pallas kernels  92.8 us (99%)
    pallas_call x1, Pallas kernels, run_whole(): pl.pallas_call(functools.partial(whole_kernel, n, groups), out_shape=(vm(...  89.8 us
    pallas_call x1, Pallas kernels, write_out(): pl.pallas_call(write_kernel, out_shape=tuple((jax.ShapeDtypeStruct(a.shap...  2.96 us

profile of v5, /device:TPU:0, one launch (start us, length us, event | category | flops | bytes accessed | tf_op | source)
XLA Modules:
  0.0 93.4 jit_solution(1530332456389749891)
XLA Ops:
  0.6 89.8 %shard_map.190 = (f32[2048,256]{1,0:T(8,128)S(1)}, f32[2048,256]{1,0:T(8,128)S(1)}, f32[256,2048]{1,0:T(8,128)S(1)}, f32[256,512]{1,0:T(8,128)S(1)}, bf16[192,51...) custom-call(bf16[192,512]{1,0:T(8,128)(2,1)} %mixed_hbm.1, bf16[192,512]{1,0:T(8,128)(2,1)} %cot_hbm.1, ...), custom_call_target="tpu_custom_call" | custom-call | flops 8000000000 | bytes 80000000 | tf_op jit(solution)/shard_map/pallas_call | solution.py:619
  90.5 3.0 %shard_map.191 = (f32[2048,256]{1,0:T(8,128)}, f32[2048,256]{1,0:T(8,128)}, f32[256,2048]{1,0:T(8,128)}, f32[256,512]{1,0:T(8,128)}, bf16[192,512]{1,0:T(8,128)(2,1)}, /*index=5*/bf16[192,512]{1,0:T(8,128)(2,1)}) custom-call(f32[2048,256]{1,0:T(8,128)S(1)} %get-tuple-element.18.refs_0_, f32[2048,256]{1,0:T(8,128)S(1)} %get-tuple-element.19.refs_1_, ...), custom_call_target="tpu_custom_call" | custom-call | tf_op jit(solution)/shard_map/pallas_call | solution.py:675

commit v6 on v5

--- a/solution.py
+++ b/solution.py
@@ -376,33 +376,46 @@
         for _ in range(min(count, len(work))):
             work.pop(0)()
 
-    line_group = per // 2
+    def ready(count):
+        if count % per:
+            return
+        g = count // per - 1
+        expert(g)
+        if g == 3:
+            join_near(0)
+        if g == 5:
+            join_near(4)
+            join_near(5)
+
+    ready(1)
     for j in range(1, lines):
-        g = j // line_group if j % line_group == 0 else 0
         arrive(j)
-        if g == 3:
-            join_far(1)
         relay(2 * j - 1)
-        if j == max(1, lines - 2) or g == 3:
+        if j == max(1, lines - 2):
             some_of(steps, 1)
-        if g:
-            expert(g - 1)
-        if g == 2:
-            join_near(1)
+        ready(2 * j)
         crossed(j)
+        if j == lines - 1:
+            some_of(steps, 1)
         relay(2 * j)
-    join_near(2)
+        ready(2 * j + 1)
+    for g in (6, 2, 3):
+        join_near(g)
+    join_far(4)
+    join_far(5)
     relay(n - 1)
+    ready(n)
+    join_near(7)
+    join_near(1)
+    for g in (6, 2, 3):
+        join_far(g)
+    some_of(grad_chunks, 3)
+    join_far(7)
+    some_of(grad_chunks, 2)
+    join_far(0)
+    join_far(1)
     some_of(steps, 1)
-    expert(3)
-    join_near(3)
-    join_near(0)
-    join_far(2)
-    some_of(grad_chunks, 4)
-    some_of(steps, 1)
-    join_far(3)
-    some_of(grad_chunks, 4)
-    join_far(0)
+    some_of(grad_chunks, 3)
     lane = lax.broadcasted_iota(jnp.int32, (tokens, 128), 1)
     away = []
     for j in range(top):
@@ -560,8 +573,7 @@
     first = dec[0:1, :]
     mine_pair[0:1, :] = prods[0:1, :] * first
     mine_pair[1:2, :] = carry * first
-    mine_pair[2:8, :] = jnp.zeros((6, total), f32)
-    pairs[me] = jnp.zeros((8, total), f32)
+    pairs[me] = jnp.zeros((2, total), f32)
 
     def pair_to(peer, source):
         return remote(mine_pair, pairs.at[source], pair_sem.at[source], {"sp": peer})
@@ -607,7 +619,7 @@
 ):
     tokens, width = mixed.shape
     full, hidden = wg.shape
-    groups = 4
+    groups = 8
     per = n // groups
     block = per * slots
     some = n // parts
@@ -645,8 +657,8 @@
             vm((n, tokens, thin), half),
             vm((some, tokens, thin), half),
             vm((some, tokens, thin), half),
-            vm((8, width), f32),
-            vm((n, 8, width), f32),
+            vm((2, width), f32),
+            vm((n, 2, width), f32),
             dma((2,)), dma((n // 2, 2)), pltpu.SemaphoreType.REGULAR, dma((n // 2, 2)), dma((n // 2,)), dma((n // 2,)), dma((n,)), dma((n,)), dma((n,)),
             dma((groups, 2)),
             dma((groups,)), dma((n,)), dma((3,)), dma((15,)),

time: 93.7 us -> 91 us (0.971)
  Pallas kernels: 92.8 us -> 89.9 us
    pallas_call x1, Pallas kernels: 89.8 us -> 86.9 us  [run_whole(): pl.pallas_call(functools.partial(whole_kernel, n, groups), out_shape=(vm(...]
where the time goes in v6:
time: 91 us; the launch traced here: 90.7 us
  Pallas kernels  89.9 us (99%)
    pallas_call x1, Pallas kernels, run_whole(): pl.pallas_call(functools.partial(whole_kernel, n, groups), out_shape=(vm(...  86.9 us
    pallas_call x1, Pallas kernels, write_out(): pl.pallas_call(write_kernel, out_shape=tuple((jax.ShapeDtypeStruct(a.shap...  2.96 us

profile of v6, /device:TPU:0, one launch (start us, length us, event | category | flops | bytes accessed | tf_op | source)
XLA Modules:
  0.0 90.7 jit_solution(5057583569199460037)
XLA Ops:
  0.6 86.9 %shard_map.190 = (f32[2048,256]{1,0:T(8,128)S(1)}, f32[2048,256]{1,0:T(8,128)S(1)}, f32[256,2048]{1,0:T(8,128)S(1)}, f32[256,512]{1,0:T(8,128)S(1)}, bf16[192,51...) custom-call(bf16[192,512]{1,0:T(8,128)(2,1)} %mixed_hbm.1, bf16[192,512]{1,0:T(8,128)(2,1)} %cot_hbm.1, ...), custom_call_target="tpu_custom_call" | custom-call | flops 8000000000 | bytes 80000000 | tf_op jit(solution)/shard_map/pallas_call | solution.py:631
  87.6 3.0 %shard_map.191 = (f32[2048,256]{1,0:T(8,128)}, f32[2048,256]{1,0:T(8,128)}, f32[256,2048]{1,0:T(8,128)}, f32[256,512]{1,0:T(8,128)}, bf16[192,512]{1,0:T(8,128)(2,1)}, /*index=5*/bf16[192,512]{1,0:T(8,128)(2,1)}) custom-call(f32[2048,256]{1,0:T(8,128)S(1)} %get-tuple-element.18.refs_0_, f32[2048,256]{1,0:T(8,128)S(1)} %get-tuple-element.19.refs_1_, ...), custom_call_target="tpu_custom_call" | custom-call | tf_op jit(solution)/shard_map/pallas_call | solution.py:687
